TPU v7x, 256 devices: a whole 4x4x8 slice. The times are simulated.
256 devices in a mesh: fs: 32 (over z, y), tp: 8 (over x, core).
Axes of the slice: x: 4, y: 4, z: 8, core: 2. Of those that a mesh axis runs over, the one named last changes fastest.
Arguments:
- latent_in: bfloat16 [98304, 512], P('fs'), may hold values from -6 to 6
- query_cot: bfloat16 [98304, 1536], P('fs', 'tp'), may hold values from -6 to 6
- attn_out: bfloat16 [98304, 1024], P('fs'), may hold values from -6 to 6
- mix_cot: bfloat16 [98304, 2048], P('fs', 'tp'), may hold values from -6 to 6
- query_weight: float32 [512, 1536], P('fs', 'tp'), may hold values from -0.25 to 0.25
- output_weight: float32 [1024, 2048], P('fs', 'tp'), may hold values from -0.1875 to 0.1875
- query_factor: bfloat16 [512, 256], P('fs'), may hold values from -0.25 to 0.25
- output_factor: bfloat16 [1024, 256], P('fs'), may hold values from -0.1875 to 0.1875
- query_mean: float32 [256, 1536], P('fs', 'tp'), may hold values from -3 to 3
- query_square: float32 [256, 1536], P('fs', 'tp'), may hold values from 0.05 to 1
- output_mean: float32 [256, 2048], P('fs', 'tp'), may hold values from -3 to 3
- output_square: float32 [256, 2048], P('fs', 'tp'), may hold values from 0.05 to 1
Outputs:
- step_query: float32 [512, 1536], P('fs', 'tp')
- step_output: float32 [1024, 2048], P('fs', 'tp')
- new_query: float32 [512, 1536], P('fs', 'tp')
- new_output: float32 [1024, 2048], P('fs', 'tp')
- copy_query: bfloat16 [512, 1536], P(None, 'tp')
- copy_output: bfloat16 [1024, 2048], P(None, 'tp')
- query_mean_new: float32 [256, 1536], P('fs', 'tp')
- query_square_new: float32 [256, 1536], P('fs', 'tp')
- output_mean_new: float32 [256, 2048], P('fs', 'tp')
- output_square_new: float32 [256, 2048], P('fs', 'tp')
All inputs are finite; a program needn't handle non-finite values.
Results may differ from a plain program's by a relative error of at most 0.0085.
Values may be sent and summed in bfloat16 or wider, within the bound.
No kernel may reach another device: no remote copies, remote signals or barrier semaphores. Data moves between devices by JAX's collectives and lax.ppermute only.
A program may use at most 64 MiB of HBM per device.

v0:
```python
import math

import jax
import jax.numpy as jnp
from jax import lax
from jax.sharding import PartitionSpec as P


def sent_to_all(x, axis):
    copies = jnp.broadcast_to(x, (lax.axis_size(axis), *x.shape))
    return lax.all_to_all(copies, axis, split_axis=0, concat_axis=0, tiled=True)


def laid_out(tiles, dim):
    dims = list(tiles.shape[1:])
    dims[dim] *= tiles.shape[0]
    return jnp.moveaxis(tiles, 0, dim).reshape(dims)


def gathered_copies(x, axis, dim):
    tiles = sent_to_all(x, axis)
    return laid_out(tiles, dim)


def cut_along(x, dim, count):
    before, after = (x.shape[:dim], x.shape[dim + 1 :])
    return jnp.moveaxis(x.reshape(*before, count, -1, *after), dim, 0)


def sent_and_summed(x, axis, dim):
    tiles = cut_along(x, dim, lax.axis_size(axis))
    arrived = lax.all_to_all(tiles, axis, split_axis=0, concat_axis=0, tiled=True)
    return arrived.sum(axis=0)


def over_copies(x, axis):
    everything = sent_to_all(x, axis)
    return jnp.sum(everything, axis=0)


def in_one(arrays, axis):
    ends = [0]
    for a in arrays:
        ends.append(ends[-1] + a.size)
    subtotal = over_copies(jnp.concatenate([a.ravel() for a in arrays]), axis)
    return tuple((subtotal[b:e].reshape(a.shape) for a, b, e in zip(arrays, ends, ends[1:])))


def one_gather(arrays, axis, dims):
    vector = jnp.concatenate([a.reshape(-1) for a in arrays])
    lines, at, outs = (lax.all_gather(vector, axis), 0, [])
    for a, dim in zip(arrays, dims):
        tiles = lines[:, at : at + a.size].reshape(-1, *a.shape)
        outs.append(laid_out(tiles, dim))
        at += a.size
    return tuple(outs)


def over_rows(left, right):
    return lax.dot_general(
        left, right, (((0,), (0,)), ((), ())), preferred_element_type=jnp.float32
    )


def over_rows_exact(left, right):
    return lax.dot_general(
        left,
        right,
        (((0,), (0,)), ((), ())),
        precision=lax.Precision.HIGHEST,
        preferred_element_type=jnp.float32,
    )


def exact_dot(left, right):
    return jnp.dot(left, right, precision=lax.Precision.HIGHEST, preferred_element_type=jnp.float32)


def moments(mean, square, low):
    mean_new = 0.8 * mean + 0.2 * low
    square_new = 0.9 * square + 0.1 * low * low
    return (mean_new, square_new, mean_new / jnp.sqrt(square_new))


def on_device(
    latent_in,
    query_cot,
    attn_out,
    mix_cot,
    query_weight,
    output_weight,
    query_factor,
    output_factor,
    query_mean,
    query_square,
    output_mean,
    output_square,
):
    tokens_local = latent_in.shape[0]
    inv_root = 1.0 / math.sqrt(tokens_local * lax.axis_size("fs"))
    weight_rows = query_weight.shape[0]
    query_width = query_weight.shape[1]
    output_width = output_weight.shape[1]
    rank = query_factor.shape[1]
    factor_query = query_factor.astype(jnp.float32)
    factor_output = output_factor.astype(jnp.float32)
    stacked = jnp.concatenate([query_factor, output_factor.reshape(weight_rows, 2 * rank)], axis=1)
    whole_factors = gathered_copies(stacked, "fs", 0).astype(jnp.float32)
    all_rows = whole_factors.shape[0]
    whole_query = whole_factors[:, :rank]
    whole_output = whole_factors[:, rank:].reshape(2 * all_rows, rank)
    partial_query = over_rows(latent_in, query_cot)
    partial_output = over_rows(attn_out, mix_cot)
    low = sent_and_summed(
        jnp.concatenate(
            [
                over_rows_exact(whole_query, partial_query),
                over_rows_exact(whole_output, partial_output),
            ],
            axis=1,
        )
        * inv_root,
        "fs",
        0,
    )
    mean_q, square_q, direction_q = moments(query_mean, query_square, low[:, :query_width])
    mean_o, square_o, direction_o = moments(output_mean, output_square, low[:, query_width:])
    joined = jnp.concatenate([direction_q, direction_o], axis=1)
    piece = gathered_copies(joined, "fs", 0)
    piece_query = piece[:, :query_width]
    piece_output = piece[:, query_width:]
    product_q = exact_dot(factor_query, piece_query)
    product_o = exact_dot(factor_output, piece_output)
    square_sum_q = jnp.sum(piece_query * piece_query)
    square_sum_o = jnp.sum(piece_output * piece_output)
    square_sum_q, square_sum_o = in_one((square_sum_q, square_sum_o), "tp")
    columns = lax.axis_size("tp")
    scale_q = 1.0 / jnp.sqrt(square_sum_q / (rank * query_width * columns) + 0.25)
    scale_o = 1.0 / jnp.sqrt(square_sum_o / (rank * output_width * columns) + 0.25)
    step_q = product_q * scale_q
    step_o = product_o * scale_o
    new_q = query_weight - 0.02 * step_q
    new_o = output_weight - 0.02 * step_o
    copy_q, copy_o = one_gather(
        (new_q.astype(jnp.bfloat16), new_o.astype(jnp.bfloat16)), "fs", (0, 0)
    )
    return (step_q, step_o, new_q, new_o, copy_q, copy_o, mean_q, square_q, mean_o, square_o)


def solution(mesh):
    placed = (
        P("fs", None),
        P("fs", "tp"),
        P("fs", None),
        P("fs", "tp"),
        P("fs", "tp"),
        P("fs", "tp"),
        P("fs", None),
        P("fs", None),
        P("fs", "tp"),
        P("fs", "tp"),
        P("fs", "tp"),
        P("fs", "tp"),
    )
    return jax.shard_map(
        on_device,
        mesh=mesh,
        in_specs=placed,
        out_specs=(
            P("fs", "tp"),
            P("fs", "tp"),
            P("fs", "tp"),
            P("fs", "tp"),
            P(None, "tp"),
            P(None, "tp"),
            P("fs", "tp"),
            P("fs", "tp"),
            P("fs", "tp"),
            P("fs", "tp"),
        ),
        check_vma=False,
    )
```

profile of v0, /device:TPU:2, one launch (start us, length us, event | category | flops | bytes accessed | tf_op | source)
XLA Modules:
  0.0 175.2 jit_solution(3181078471940393403)
XLA Ops:
  0.7 0.9 reshape.64
  1.5 0.8 pad_maximum_fusion
  2.3 0.9 broadcast_in_dim.9
  3.3 11.6 %all-to-all-start = ((bf16[32,16,768]{2,1,0:T(8,128)(2,1)}), bf16[32,16,768]{2,1,0:T(8,128)(2,1)}, u32[]{:S(2)}, u32[]{:S(2)}) async-start(bf16[32,16,768]{2,1,0:T(8,128)(2,1)} %broadcast_in_dim.9), calls=%async_computation | async-start | bytes 1572864 | tf_op jit(solution)/shard_map/all_to_all | solution.py:11
  14.9 2.2 %fusion.13 = f32[512,192]{0,1:T(8,128)S(1)} fusion(bf16[3072,192]{0,1:T(8,128)(2,1)} %param.13, bf16[3072,512]{1,0:T(8,128)(2,1)S(1)} %copy-done), kind=kOutput, calls=%fused_computation.31 | convolution fusion | flops 603979776 | bytes 4718592 | tf_op jit(solution)/shard_map/dot_general | solution.py:60
  17.1 5.6 %convolution_bitcast_fusion = f32[1024,256,1]{1,0,2:T(8,128)} fusion(bf16[3072,1024]{1,0:T(8,128)(2,1)} %param.14, bf16[3072,256]{1,0:T(8,128)(2,1)S(1)} %copy-done.2), kind=kOutput, calls=%fused_computation | convolution fusion | flops 1610612736 | bytes 8912896 | tf_op jit(solution)/shard_map/dot_general | solution.py:60
  22.7 15.1 %all-to-all-done = bf16[32,16,768]{2,1,0:T(8,128)(2,1)} async-done(((bf16[32,16,768]{2,1,0:T(8,128)(2,1)}), bf16[32,16,768]{2,1,0:T(8,128)(2,1)}, u32[]{:S(2)}, u32[]{:S(2)}) %all-to-all-start) | async-done | bytes 786464 | tf_op jit(solution)/shard_map/all_to_all | solution.py:11
  37.7 1.9 %slice.41 = bf16[512,512]{1,0:T(8,128)(2,1)} slice(bf16[512,768]{1,0:T(8,128)(2,1)} %bitcast), slice={[0:512], [256:768]} | slice | bytes 1048576 | tf_op jit(solution)/shard_map/slice | solution.py:111
  39.6 2.1 %convolution_bitcast_fusion.1 = f32[32,8,192]{2,1,0:T(8,128)} fusion(f32[512,192]{0,1:T(8,128)S(1)} %fusion.13, bf16[512,768]{1,0:T(8,128)(2,1)} %bitcast), kind=kOutput, calls=%fused_computation.1 | convolution fusion | flops 301989888 | bytes 851968 | tf_op jit(solution)/shard_map/dot_general | solution.py:66
  41.7 2.1 %reshape.66 = bf16[1024,256]{1,0:T(8,128)(2,1)} reshape(bf16[512,512]{1,0:T(8,128)(2,1)} %slice.41) | data formatting | bytes 1048576 | tf_op jit(solution)/shard_map/reshape | solution.py:111
  43.8 2.0 %copy.45 = bf16[256,1024]{1,0:T(8,128)(2,1)} copy(bf16[256,1024]{0,1:T(8,128)(2,1)} %bitcast.33) | data formatting | bytes 1048576 | tf_op jit(solution)/shard_map/dot_general | solution.py:66
  45.8 2.1 %fusion.2 = f32[32,8,256]{2,1,0:T(8,128)S(1)} fusion(f32[1024,256,1]{1,0,2:T(8,128)} %convolution_bitcast_fusion, bf16[256,1024]{1,0:T(8,128)(2,1)} %copy.45), kind=kOutput, calls=%fused_computation.7 | convolution fusion | flops 805306368 | bytes 1835008 | tf_op jit(solution)/shard_map/dot_general | solution.py:66
  48.2 21.7 %all_to_all.21 = f32[32,8,448]{2,1,0:T(8,128)} all-to-all(f32[32,8,448]{2,1,0:T(8,128)S(1)} %maximum_multiply_fusion), channel_id=1, replica_groups=mesh['fs'=32,'tp'=8] {'fs'}, dimensions={0} | all-to-all | bytes 917504 | tf_op jit(solution)/shard_map/all_to_all | solution.py:32
  69.9 1.1 reduce_sum.36
  71.0 0.7 rsqrt_multiply_fusion
  71.7 0.6 rsqrt_multiply_fusion.1
  72.4 21.0 %all_to_all.22 = f32[32,8,448]{2,1,0:T(8,128)S(1)} all-to-all(f32[32,8,448]{2,1,0:T(8,128)S(1)} %broadcast_in_dim.10), channel_id=1, replica_groups=mesh['fs'=32,'tp'=8] {'fs'}, dimensions={0} | all-to-all | bytes 917504 | tf_op jit(solution)/shard_map/all_to_all | solution.py:11
  93.5 0.7 multiply_reduce_fusion
  94.3 0.8 copy.51
  95.1 1.6 multiply_reduce_fusion.1
  96.7 1.4 pad_maximum_fusion.3
  98.0 8.5 %all_to_all.23 = f32[8,1,2]{2,1,0:T(1,128)S(1)} all-to-all(f32[8,1,2]{2,1,0:T(1,128)S(1)} %broadcast_in_dim.11), channel_id=1, replica_groups=mesh['fs'=32,'tp'=8] {'tp'}, dimensions={0} | all-to-all | bytes 128 | tf_op jit(solution)/shard_map/all_to_all | solution.py:11
  108.5 1.3 fusion
  109.8 1.8 %fusion.9 = (bf16[16,192]{1,0:T(8,128)(2,1)S(1)}, f32[16,192]{1,0:T(8,128)}, f32[16,192]{1,0:T(8,128)}) fusion(f32[16,192]{1,0:T(8,128)S(1)} %copy-done.8, f32[]{:T(128)} %bitcast.8, bf16[16,256]{1,0:T(8,128)(2,1)S(1)} %copy-done.7, f32[256,448]{1,0:T(8,128)} %bitcast.32), kind=kOutput, calls=%fused_computation.29 | convolution fusion | flops 9449472 | bytes 313856 | tf_op jit(solution)/shard_map/dot_general | solution.py:76
  111.7 0.6 convert_bitcast_fusion
  112.4 53.0 %all-gather = bf16[360448]{0:T(1024)(128)(2,1)} all-gather(bf16[11264]{0:T(1024)(128)(2,1)S(1)} %pad_maximum_fusion.1), channel_id=2, replica_groups=mesh['fs'=32,'tp'=8] {'fs'}, dimensions={0}, use_global_device_ids=true | all-gather | bytes 743424 | tf_op jit(solution)/shard_map/all_gather | solution.py:51
  165.4 2.1 %reshape.72 = bf16[32,11264]{1,0:T(8,128)(2,1)} reshape(bf16[360448]{0:T(1024)(128)(2,1)} %all-gather) | data formatting | bytes 1441792 | tf_op jit(solution)/shard_map/all_gather | solution.py:51
  167.5 1.6 slice.46
  169.2 1.9 %slice.47 = bf16[32,8192]{1,0:T(8,128)(2,1)} slice(bf16[32,11264]{1,0:T(8,128)(2,1)} %reshape.72), slice={[0:32], [3072:11264]} | slice | bytes 1048576 | tf_op jit(solution)/shard_map/slice | solution.py:53
  171.0 2.1 %reshape_reshape.7 = bf16[1024,256]{1,0:T(8,128)(2,1)} reshape(bf16[32,8192]{1,0:T(8,128)(2,1)} %slice.47) | data formatting | bytes 1048576 | tf_op jit(solution)/shard_map/reshape;reshape | solution.py:17
  173.1 1.2 reshape_reshape.6
  174.4 0.8 copy.48
  (36 shorter events, 1.2 us)
Async XLA Ops:
  0.6 14.2 %copy-start = (bf16[3072,512]{1,0:T(8,128)(2,1)S(1)}, bf16[3072,512]{1,0:T(8,128)(2,1)}, u32[]{:S(2)}) copy-start(bf16[3072,512]{1,0:T(8,128)(2,1)} %param.12) | copy-start | bytes 9437188
  3.3 34.5 %all-to-all-start = ((bf16[32,16,768]{2,1,0:T(8,128)(2,1)}), bf16[32,16,768]{2,1,0:T(8,128)(2,1)}, u32[]{:S(2)}, u32[]{:S(2)}) async-start(bf16[32,16,768]{2,1,0:T(8,128)(2,1)} %broadcast_in_dim.9), calls=%async_computation | async-start | bytes 1572864 | tf_op jit(solution)/shard_map/all_to_all | solution.py:11
  14.9 2.2 %copy-start.2 = (bf16[3072,256]{1,0:T(8,128)(2,1)S(1)}, bf16[3072,256]{1,0:T(8,128)(2,1)}, u32[]{:S(2)}) copy-start(bf16[3072,256]{1,0:T(8,128)(2,1)} %param.15) | copy-start | bytes 4718596
  41.7 6.2 %copy-start.3 = (f32[32,8,192]{2,1,0:T(8,128)S(1)}, f32[32,8,192]{2,1,0:T(8,128)}, u32[]{:S(2)}) copy-start(f32[32,8,192]{2,1,0:T(8,128)} %convolution_bitcast_fusion.1) | copy-start | bytes 589828
  41.7 29.3 %copy-start.9 = (f32[8,256]{1,0:T(8,128)S(1)}, f32[8,256]{1,0:T(8,128)}, u32[]{:S(2)}) copy-start(f32[8,256]{1,0:T(8,128)} %param.23) | copy-start | bytes 24580
  41.7 29.3 %copy-start.10 = (f32[8,256]{1,0:T(8,128)S(1)}, f32[8,256]{1,0:T(8,128)}, u32[]{:S(2)}) copy-start(f32[8,256]{1,0:T(8,128)} %param.22) | copy-start | bytes 24580
  41.7 30.0 %copy-start.11 = (f32[8,192]{1,0:T(8,128)S(1)}, f32[8,192]{1,0:T(8,128)}, u32[]{:S(2)}) copy-start(f32[8,192]{1,0:T(8,128)} %param.21) | copy-start | bytes 18436
  41.7 30.0 %copy-start.12 = (f32[8,192]{1,0:T(8,128)S(1)}, f32[8,192]{1,0:T(8,128)}, u32[]{:S(2)}) copy-start(f32[8,192]{1,0:T(8,128)} %param.20) | copy-start | bytes 18436
  47.9 60.6 %copy-start.5 = (bf16[32,256]{1,0:T(8,128)(2,1)S(1)}, bf16[32,256]{1,0:T(8,128)(2,1)}, u32[]{:S(2)}) copy-start(bf16[32,256]{1,0:T(8,128)(2,1)} %param.19) | copy-start | bytes 49156
  47.9 61.9 %copy-start.7 = (bf16[16,256]{1,0:T(8,128)(2,1)S(1)}, bf16[16,256]{1,0:T(8,128)(2,1)}, u32[]{:S(2)}) copy-start(bf16[16,256]{1,0:T(8,128)(2,1)} %param.18) | copy-start | bytes 24580
  48.0 61.9 %copy-start.8 = (f32[16,192]{1,0:T(8,128)S(1)}, f32[16,192]{1,0:T(8,128)}, u32[]{:S(2)}) copy-start(f32[16,192]{1,0:T(8,128)} %param.16) | copy-start | bytes 36868
  48.0 63.8 %copy-start.6 = (f32[32,256]{1,0:T(8,128)S(1)}, f32[32,256]{1,0:T(8,128)}, u32[]{:S(2)}) copy-start(f32[32,256]{1,0:T(8,128)} %param.17) | copy-start | bytes 98308
  93.5 0.8 copy-start.1
  109.8 65.3 %copy-start.4 = (f32[32,256]{1,0:T(8,128)}, f32[32,256]{1,0:T(8,128)S(1)}, u32[]{:S(2)}) copy-start(f32[32,256]{1,0:T(8,128)S(1)} %fusion) | copy-start | bytes 98308
where the time goes:
time: 176 us; the launch traced here: 175 us
  blocking collectives  104 us (59%)
  local copies, waits for them, and re-layouts  19.2 us (11%)
  matrix products  15.1 us (9%)
  waiting for transfers between devices  15.1 us (9%)
  starting transfers between devices  11.6 us (7%)
  other arithmetic  7.72 us (4%)
  between operations  2.24 us (1%)
    all_gather x1, blocking collectives, one_gather(): lines, at, outs = (lax.all_gather(vector, axis), 0, [])  53 us
    all_to_all x2, blocking collectives, sent_to_all(): return lax.all_to_all(copies, axis, split_axis=0, concat_axis=0, tiled=True)  29.5 us
    all_to_all x1, blocking collectives, sent_and_summed(): lax.all_to_all(tiles, axis, split_axis=0, concat_axis=0, tiled=True)  21.7 us
    all_to_all x1, waiting for transfers between devices, sent_to_all(): return lax.all_to_all(copies, axis, split_axis=0, concat_axis=0, tiled=True)  15.1 us
    all_to_all x1, starting transfers between devices, sent_to_all(): return lax.all_to_all(copies, axis, split_axis=0, concat_axis=0, tiled=True)  11.6 us
    dot_general x2, matrix products, over_rows(): lax.dot_general(left, right, (((0,), (0,)), ((), ())), preferred_element_...  7.78 us
    dot_general x2, matrix products, over_rows_exact(): lax.dot_general(left, right, (((0,), (0,)), ((), ())), precision=lax.Prec...  4.18 us
  transfers between devices with their start and end apart: 1, of which 1 were waited for; matrix products, arithmetic and copies ran while one was open for 4% of the time, Pallas kernels for 0%

commit v1 on v0

v1 whole, which is shorter than its diff:
```python
import math

import jax
import jax.numpy as jnp
from jax import lax
from jax.sharding import PartitionSpec as P


def exchange(tiles, axis):
    return lax.all_to_all(tiles, axis, split_axis=0, concat_axis=0, tiled=True)


def sent_to_all(x, axis):
    return exchange(jnp.broadcast_to(x, (lax.axis_size(axis), *x.shape)), axis)


def contract(left, right, dims):
    return lax.dot_general(left, right, (dims, ((), ())), preferred_element_type=jnp.float32)


def moments(mean, square, low):
    mean_new = 0.8 * mean + 0.2 * low
    square_new = 0.9 * square + 0.1 * low * low
    return (mean_new, square_new, mean_new / jnp.sqrt(square_new))


def on_device(
    latent_in,
    query_cot,
    attn_out,
    mix_cot,
    query_weight,
    output_weight,
    query_factor,
    output_factor,
    query_mean,
    query_square,
    output_mean,
    output_square,
):
    bf16 = jnp.bfloat16
    count = lax.axis_size("fs")
    columns = lax.axis_size("tp")
    inv_root = 1.0 / math.sqrt(latent_in.shape[0] * count)
    rows_q, width_q = query_weight.shape
    rows_o, width_o = output_weight.shape
    rank = query_factor.shape[1]

    factors = sent_to_all(jnp.concatenate([query_factor, output_factor], axis=0), "fs")
    padded = jnp.pad(query_weight.astype(bf16), ((0, 0), (0, width_o - width_q)))
    weights = sent_to_all(jnp.concatenate([padded, output_weight.astype(bf16)], axis=0), "fs")

    grad_q = contract(latent_in, query_cot, ((0,), (0,))).astype(bf16)
    grad_o = contract(attn_out, mix_cot, ((0,), (0,))).astype(bf16)
    factor_q = factors[:, :rows_q].reshape(count * rows_q, rank)
    factor_o = factors[:, rows_q:].reshape(count * rows_o, rank)
    low = jnp.concatenate(
        [contract(factor_q, grad_q, ((0,), (0,))), contract(factor_o, grad_o, ((0,), (0,)))], axis=1
    )
    low = (low * inv_root).astype(bf16).reshape(count, rank // count, width_q + width_o)
    low = jnp.sum(exchange(low, "fs").astype(jnp.float32), axis=0)

    mean_q, square_q, direction_q = moments(query_mean, query_square, low[:, :width_q])
    mean_o, square_o, direction_o = moments(output_mean, output_square, low[:, width_q:])
    joined = jnp.concatenate([direction_q, direction_o], axis=1).astype(bf16)
    piece = sent_to_all(joined, "fs").reshape(rank, width_q + width_o)
    piece_q, piece_o = piece[:, :width_q], piece[:, width_q:]

    squares = jnp.sum(jnp.square(piece.astype(jnp.float32)), axis=0)
    sums = jnp.stack([jnp.sum(squares[:width_q]), jnp.sum(squares[width_q:])])
    sums = jnp.sum(sent_to_all(sums.reshape(1, 2), "tp"), axis=0)[0]
    scale_q = 1.0 / jnp.sqrt(sums[0] / (rank * width_q * columns) + 0.25)
    scale_o = 1.0 / jnp.sqrt(sums[1] / (rank * width_o * columns) + 0.25)

    step_q = contract(query_factor, piece_q, ((1,), (0,))) * scale_q
    step_o = contract(output_factor, piece_o, ((1,), (0,))) * scale_o
    new_q = query_weight - 0.02 * step_q
    new_o = output_weight - 0.02 * step_o

    whole_q = weights[:, :rows_q, :width_q].reshape(count * rows_q, width_q)
    whole_o = weights[:, rows_q:].reshape(count * rows_o, width_o)
    step_all_q = contract(factor_q, piece_q, ((1,), (0,))) * scale_q
    step_all_o = contract(factor_o, piece_o, ((1,), (0,))) * scale_o
    copy_q = (whole_q.astype(jnp.float32) - 0.02 * step_all_q).astype(bf16)
    copy_o = (whole_o.astype(jnp.float32) - 0.02 * step_all_o).astype(bf16)
    return (step_q, step_o, new_q, new_o, copy_q, copy_o, mean_q, square_q, mean_o, square_o)


def solution(mesh):
    rows = P("fs", None)
    both = P("fs", "tp")
    gathered = P(None, "tp")
    return jax.shard_map(
        on_device,
        mesh=mesh,
        in_specs=(rows, both, rows, both, both, both, rows, rows, both, both, both, both),
        out_specs=(both, both, both, both, gathered, gathered, both, both, both, both),
        check_vma=False,
    )
```

time: 176 us -> 137 us (0.78)
  waiting for transfers between devices: 15.1 us -> 0 us
  starting transfers between devices: 11.6 us -> 0 us
  local copies, waits for them, and re-layouts: 19.2 us -> 10.5 us
  blocking collectives: 104 us -> 101 us
    all_gather x1 -> x0, blocking collectives: 53 us -> none  [one_gather(): lines, at, outs = (lax.all_gather(vector, axis), 0, [])]
    all_to_all x3 -> x5, blocking collectives: 51.2 us -> 101 us  [exchange(): return lax.all_to_all(tiles, axis, split_axis=0, concat_axis=0, tiled=True)]
    all_to_all x1 -> x0, waiting for transfers between devices: 15.1 us -> none  [sent_to_all(): return lax.all_to_all(copies, axis, split_axis=0, concat_axis=0, tiled=True)]
    all_to_all x1 -> x0, starting transfers between devices: 11.6 us -> none  [sent_to_all(): return lax.all_to_all(copies, axis, split_axis=0, concat_axis=0, tiled=True)]
    another operation x2 -> x0, local copies, waits for them, and re-layouts: 3.32 us -> none  [laid_out(): return jnp.moveaxis(tiles, 0, dim).reshape(dims)]
    reshape x3 -> x0, local copies, waits for them, and re-layouts: 3.03 us -> none  [the longest x1 2.06 us: on_device(): whole_output = whole_factors[:, rank:].reshape(2 * all_rows, rank)]
    another operation x0 -> x3, other arithmetic: none -> 2.65 us  [the longest x1 1.37 us: on_device(): sums = jnp.stack([jnp.sum(squares[:width_q]), jnp.sum(squares[width_q:])])]
    slice x4 -> x5, local copies, waits for them, and re-layouts: 5.94 us -> 3.63 us  [the longest x1 1.88 us: on_device(): factor_o = factors[:, rows_q:].reshape(count * rows_o, rank)]
  transfers between devices with their start and end apart: 1 -> 0, of which waited for: 1 -> 0; matrix products, arithmetic and copies ran while one was open for 4% -> 0% of each run, Pallas kernels for 0% -> 0%
where the time goes in v1:
time: 137 us; the launch traced here: 136 us
  blocking collectives  101 us (74%)
  matrix products  15 us (11%)
  local copies, waits for them, and re-layouts  10.5 us (8%)
  other arithmetic  7.08 us (5%)
  between operations  2.16 us (2%)
    all_to_all x5, blocking collectives, exchange(): return lax.all_to_all(tiles, axis, split_axis=0, concat_axis=0, tiled=True)  101 us
    dot_general x6, matrix products, contract(): lax.dot_general(left, right, (dims, ((), ())), preferred_element_type=jnp...  15 us
    dot_general x2, local copies, waits for them, and re-layouts, contract(): lax.dot_general(left, right, (dims, ((), ())), preferred_element_type=jnp...  2.9 us

profile of v1, /device:TPU:2, one launch (start us, length us, event | category | flops | bytes accessed | tf_op | source)
XLA Modules:
  0.0 135.9 jit_solution(2961255339405247049)
XLA Ops:
  0.7 0.9 pad_maximum_fusion
  1.5 0.1 broadcast_in_dim.12
  1.6 34.3 %all_to_all.25 = bf16[32,48,256]{2,1,0:T(8,128)(2,1)S(1)} all-to-all(bf16[32,48,256]{2,1,0:T(8,128)(2,1)S(1)} %broadcast_in_dim.12), channel_id=1, replica_groups=mesh['fs'=32,'tp'=8] {'fs'}, dimensions={0} | all-to-all | bytes 1572864 | tf_op jit(solution)/shard_map/all_to_all | solution.py:10
  35.9 0.9 copy-done.2
  36.8 0.9 copy.31
  37.7 1.9 %slice.51 = bf16[32,32,256]{2,1,0:T(8,128)(2,1)} slice(bf16[32,48,256]{2,1,0:T(8,128)(2,1)} %copy-done.2), slice={[0:32], [16:48], [0:256]} | slice | bytes 1048576 | tf_op jit(solution)/shard_map/slice | solution.py:56
  39.5 2.0 %copy.32 = bf16[256,1024]{1,0:T(8,128)(2,1)} copy(bf16[256,1024]{0,1:T(8,128)(2,1)} %bitcast.49) | data formatting | bytes 1048576 | tf_op jit(solution)/shard_map/dot_general | solution.py:18
  41.6 3.0 %fusion.9 = f32[32,8,192]{2,1,0:T(8,128)} fusion(bf16[3072,192]{0,1:T(8,128)(2,1)} %param.13, bf16[3072,512]{1,0:T(8,128)(2,1)S(1)} %copy-done, bf16[256,512]{1,0:T(8,128)(2,1)} %copy.31), kind=kOutput, calls=%fused_computation.14 | convolution fusion | flops 654409728 | bytes 4784128 | tf_op jit(solution)/shard_map/dot_general | solution.py:18
  44.7 6.3 %fusion.11 = f32[32,8,256]{2,1,0:T(8,128)} fusion(bf16[3072,1024]{1,0:T(8,128)(2,1)} %param.14, bf16[3072,256]{1,0:T(8,128)(2,1)} %param.15, bf16[256,1024]{1,0:T(8,128)(2,1)} %copy.32), kind=kOutput, calls=%fused_computation.17 | convolution fusion | flops 1745092608 | bytes 8650752 | tf_op jit(solution)/shard_map/dot_general | solution.py:18
  51.0 1.2 fusion.12
  52.2 17.0 %all_to_all.26 = bf16[32,8,448]{2,1,0:T(8,128)(2,1)S(1)} all-to-all(bf16[32,8,448]{2,1,0:T(8,128)(2,1)S(1)} %fusion.12), channel_id=1, replica_groups=mesh['fs'=32,'tp'=8] {'fs'}, dimensions={0} | all-to-all | bytes 458752 | tf_op jit(solution)/shard_map/all_to_all | solution.py:10
  69.2 0.1 convert_reduce_fusion
  69.2 0.7 multiply_convert_fusion
  69.9 0.6 multiply_convert_fusion.1
  70.5 0.1 pad_maximum_fusion.1
  70.6 14.9 %all_to_all.27 = bf16[32,8,448]{2,1,0:T(8,128)(2,1)S(1)} all-to-all(bf16[32,8,448]{2,1,0:T(8,128)(2,1)S(1)} %broadcast_in_dim.13), channel_id=1, replica_groups=mesh['fs'=32,'tp'=8] {'fs'}, dimensions={0} | all-to-all | bytes 458752 | tf_op jit(solution)/shard_map/all_to_all | solution.py:10
  85.5 0.1 multiply_reduce_fusion
  85.6 0.7 slice_reduce_fusion
  86.3 0.6 slice_reduce_fusion.1
  86.9 1.4 %pad_maximum_fusion.2 = f32[2]{0:T(128)S(1)} fusion(f32[1]{0:T(128)} %bitcast.10, f32[1]{0:T(128)} %bitcast.9), kind=kLoop, calls=%fused_computation.46 | loop fusion | flops 2 | bytes 16 | tf_op jit(solution)/shard_map/stack | solution.py:70
  88.3 8.5 %all_to_all.28 = f32[8,1,2]{2,1,0:T(1,128)S(1)} all-to-all(f32[8,1,2]{2,1,0:T(1,128)S(1)} %broadcast_in_dim.14), channel_id=1, replica_groups=mesh['fs'=32,'tp'=8] {'tp'}, dimensions={0} | all-to-all | bytes 128 | tf_op jit(solution)/shard_map/all_to_all | solution.py:10
  96.8 0.6 fusion.27
  98.7 0.8 fusion.26
  99.5 0.9 fusion.25
  100.4 0.1 broadcast_in_dim.15
  100.4 26.5 %all_to_all.29 = bf16[32,48,256]{2,1,0:T(8,128)(2,1)S(1)} all-to-all(bf16[32,48,256]{2,1,0:T(8,128)(2,1)S(1)} %broadcast_in_dim.15), channel_id=1, replica_groups=mesh['fs'=32,'tp'=8] {'fs'}, dimensions={0} | all-to-all | bytes 1572864 | tf_op jit(solution)/shard_map/all_to_all | solution.py:10
  127.0 0.9 copy-done.1
  127.9 0.8 bitcast_convert_fusion
  128.7 2.0 %copy.34 = f32[512,192]{0,1:T(8,128)} copy(f32[512,192]{1,0:T(8,128)} %bitcast_convert_fusion) | data formatting | bytes 786432 | tf_op jit(solution)/shard_map/convert_element_type | solution.py:84
  130.7 1.1 slice.57
  131.8 2.2 %fusion.2 = bf16[1024,256]{1,0:T(8,128)(2,1)} fusion(bf16[1024,256]{1,0:T(8,128)(2,1)} %bitcast.50, bf16[1024,256]{1,0:T(8,128)(2,1)S(1)} %bitcast.51, f32[]{:T(128)} %bitcast.14, bf16[256,448]{1,0:T(8,128)(2,1)S(1)} %bitcast.45), kind=kOutput, calls=%fused_computation.4 | convolution fusion | flops 135528448 | bytes 1703940 | tf_op jit(solution)/shard_map/dot_general | solution.py:18
  134.1 1.9 %fusion.6 = bf16[512,192]{0,1:T(8,128)(2,1)} fusion(f32[512,192]{0,1:T(8,128)S(1)} %copy-done.4, bf16[512,256]{1,0:T(8,128)(2,1)} %bitcast.48, f32[]{:T(128)} %bitcast.12, bf16[256,448]{1,0:T(8,128)(2,1)S(1)} %bitcast.46), kind=kOutput, calls=%fused_computation.10 | convolution fusion | flops 50724864 | bytes 983044 | tf_op jit(solution)/shard_map/dot_general | solution.py:18
  (30 shorter events, 0.2 us)
Async XLA Ops:
  0.6 41.0 %copy-start = (bf16[3072,512]{1,0:T(8,128)(2,1)S(1)}, bf16[3072,512]{1,0:T(8,128)(2,1)}, u32[]{:S(2)}) copy-start(bf16[3072,512]{1,0:T(8,128)(2,1)} %param.12) | copy-start | bytes 9437188
  35.9 0.9 copy-start.2
  36.8 7.8 %copy-start.3 = (bf16[32,16,256]{2,1,0:T(8,128)(2,1)}, bf16[32,16,256]{2,1,0:T(8,128)(2,1)S(1)}, u32[]{:S(2)}) copy-start(bf16[32,16,256]{2,1,0:T(8,128)(2,1)S(1)} %slice.50) | copy-start | bytes 786436
  44.6 24.6 %copy-start.9 = (f32[8,256]{1,0:T(8,128)S(1)}, f32[8,256]{1,0:T(8,128)}, u32[]{:S(2)}) copy-start(f32[8,256]{1,0:T(8,128)} %param.23) | copy-start | bytes 24580
  44.6 24.6 %copy-start.10 = (f32[8,256]{1,0:T(8,128)S(1)}, f32[8,256]{1,0:T(8,128)}, u32[]{:S(2)}) copy-start(f32[8,256]{1,0:T(8,128)} %param.22) | copy-start | bytes 24580
  44.6 25.3 %copy-start.11 = (f32[8,192]{1,0:T(8,128)S(1)}, f32[8,192]{1,0:T(8,128)}, u32[]{:S(2)}) copy-start(f32[8,192]{1,0:T(8,128)} %param.21) | copy-start | bytes 18436
  44.6 25.3 %copy-start.12 = (f32[8,192]{1,0:T(8,128)S(1)}, f32[8,192]{1,0:T(8,128)}, u32[]{:S(2)}) copy-start(f32[8,192]{1,0:T(8,128)} %param.20) | copy-start | bytes 18436
  44.7 54.1 %copy-start.6 = (bf16[16,256]{1,0:T(8,128)(2,1)S(1)}, bf16[16,256]{1,0:T(8,128)(2,1)}, u32[]{:S(2)}) copy-start(bf16[16,256]{1,0:T(8,128)(2,1)} %param.18) | copy-start | bytes 24580
  44.7 54.1 %copy-start.8 = (f32[16,192]{1,0:T(8,128)S(1)}, f32[16,192]{1,0:T(8,128)}, u32[]{:S(2)}) copy-start(f32[16,192]{1,0:T(8,128)} %param.16) | copy-start | bytes 36868
  44.7 54.8 %copy-start.5 = (bf16[32,256]{1,0:T(8,128)(2,1)S(1)}, bf16[32,256]{1,0:T(8,128)(2,1)}, u32[]{:S(2)}) copy-start(bf16[32,256]{1,0:T(8,128)(2,1)} %param.19) | copy-start | bytes 49156
  44.7 54.8 %copy-start.7 = (f32[32,256]{1,0:T(8,128)S(1)}, f32[32,256]{1,0:T(8,128)}, u32[]{:S(2)}) copy-start(f32[32,256]{1,0:T(8,128)} %param.17) | copy-start | bytes 98308
  127.0 0.9 copy-start.1
  130.7 3.4 %copy-start.4 = (f32[512,192]{0,1:T(8,128)S(1)}, f32[512,192]{0,1:T(8,128)}, u32[]{:S(2)}) copy-start(f32[512,192]{0,1:T(8,128)} %copy.34) | copy-start | bytes 1179652

commit v2 on v1

v2 whole, which is shorter than its diff:
```python
import functools
import math

import jax
import jax.numpy as jnp
from jax import lax
from jax.experimental import pallas as pl
from jax.experimental.pallas import tpu as pltpu
from jax.sharding import PartitionSpec as P

BF16 = jnp.bfloat16
F32 = jnp.float32
LANES = 128
RING = 4


def exchange(tiles, axis):
    return lax.all_to_all(tiles, axis, split_axis=0, concat_axis=0, tiled=True)


def contract(left, right, left_dim, right_dim):
    dims = (((left_dim,), (right_dim,)), ((), ()))
    return lax.dot_general(left, right, dims, preferred_element_type=F32)


def on_chip(body, outs, *args, scratch=()):
    vmem = pl.BlockSpec(memory_space=pltpu.VMEM)
    return pl.pallas_call(
        body,
        out_shape=tuple(jax.ShapeDtypeStruct(s, d) for s, d in outs),
        in_specs=[vmem] * len(args),
        out_specs=tuple(vmem for _ in outs),
        scratch_shapes=list(scratch),
    )(*args)


def halves(x):
    return x[:, :LANES], x[:, LANES:]


def pack_body(fq, fo, wq, wo, out):
    count = out.shape[0]
    core = lax.axis_index("tp") % 2
    rows_q, rows_o = fq.shape[0], fo.shape[0]
    rows = rows_q + rows_o
    for f, at in ((fq, 0), (fo, rows_q)):
        left, right = halves(f[...])
        half = jnp.where(core == 0, left.astype(F32), right.astype(F32)).astype(BF16)
        out[:, at : at + f.shape[0]] = jnp.broadcast_to(half, (count, *half.shape))
    width_q = wq.shape[1]
    for y in range(RING):
        row, col = y % 2, y // 2
        part = wq[8 * row : 8 * row + 8, col * LANES : min(width_q, (col + 1) * LANES)]
        if part.shape[1] < LANES:
            part = jnp.concatenate([part, jnp.zeros((8, LANES - part.shape[1]), F32)], axis=1)
        left, right = halves(wo[8 * y : 8 * y + 8, :])
        quarter = jnp.concatenate([part, left, right], axis=0).astype(BF16)
        for z in range(count // RING):
            out[z * RING + y, rows:] = quarter


def low_body(inv_root, rows_q, rows, own, other, gq_t, go, out):
    count = own.shape[0]
    core = lax.axis_index("tp") % 2
    width_q = gq_t.shape[0]
    part = (count // 2, LANES * 2 // count, -1)
    for ref, at in ((own, core), (other, 1 - core)):
        fq = ref[:, :rows_q].reshape(count * rows_q, LANES)
        fo = ref[:, rows_q:rows].reshape(count * (rows - rows_q), LANES)
        low_q = contract(gq_t[...], fq, 1, 0).T * inv_root
        low_o = contract(fo, go[...], 0, 0) * inv_root
        to = pl.ds(at * (count // 2), count // 2)
        out[to, :, :width_q] = low_q.reshape(part).astype(BF16)
        out[to, :, width_q:] = low_o.reshape(part).astype(BF16)


def moments_body(parts, mq, sq, mo, so, mq_new, sq_new, mo_new, so_new, out):
    low = jnp.sum(parts[...].astype(F32), axis=0)
    width_q = mq.shape[1]
    count = out.shape[0]
    for piece, mean, square, mean_out, square_out, at in (
        (low[:, :width_q], mq, sq, mq_new, sq_new, slice(0, width_q)),
        (low[:, width_q:], mo, so, mo_new, so_new, slice(width_q, None)),
    ):
        mean_new = 0.8 * mean[...] + 0.2 * piece
        square_new = 0.9 * square[...] + 0.1 * piece * piece
        mean_out[...] = mean_new
        square_out[...] = square_new
        direction = (mean_new / jnp.sqrt(square_new)).astype(BF16)
        out[:, :, at] = jnp.broadcast_to(direction, (count, *direction.shape))


def sums_body(width_q, piece, out):
    x = piece[...].astype(F32)
    squares = jnp.sum(jnp.sum(x * x, axis=0), axis=0, keepdims=True)
    half = (out.shape[0], out.shape[1] // 2, out.shape[2])
    out[:, : half[1]] = jnp.broadcast_to(jnp.sum(squares[:, :width_q], keepdims=True)[None], half)
    out[:, half[1] :] = jnp.broadcast_to(jnp.sum(squares[:, width_q:], keepdims=True)[None], half)


def final_body(
    sizes, own, other, w0, w1, w2, w3, piece, sums, fq_own, fo_own, wq, wo,
    step_q, step_o, new_q, new_o, copy_q_t, copy_o, held_q, held_o,
):
    core = lax.axis_index("tp") % 2
    y = lax.axis_index("fs") % RING
    rows_q, width_q = wq.shape
    rows = rows_q + wo.shape[0]
    count = own.shape[0]
    for k, ref in enumerate((w0, w1, w2, w3)):
        u = (y + (RING - k)) % RING
        got = ref[...].astype(F32)
        held_q[u // 2, :, u % 2] = got[:, 0:8]
        held_o[0, :, u] = got[:, 8:16]
        held_o[1, :, u] = got[:, 16:24]
    total = jnp.sum(sums[...], axis=0)
    middle = total.shape[0] // 2
    scale_q = 1.0 / jnp.sqrt(total[0:1, :1] / sizes[0] + 0.25)
    scale_o = 1.0 / jnp.sqrt(total[middle : middle + 1, :1] / sizes[1] + 0.25)
    rank = fq_own.shape[1]
    whole = piece[...].reshape(rank, -1)
    for f, w, step, new, scale, direction in (
        (fq_own, wq, step_q, new_q, scale_q, whole[:, :width_q]),
        (fo_own, wo, step_o, new_o, scale_o, whole[:, width_q:]),
    ):
        step_own = contract(f[...], direction, 1, 0) * scale
        step[...] = step_own
        new[...] = w[...] - 0.02 * step_own
    step_all_q = 0.0
    step_all_o = 0.0
    for ref, at in ((own, core), (other, 1 - core)):
        direction = piece[pl.ds(at * (count // 2), count // 2)].reshape(LANES, -1)
        fq = ref[:, :rows_q].reshape(count * rows_q, LANES)
        fo = ref[:, rows_q:rows].reshape(count * (rows - rows_q), LANES)
        step_all_q = step_all_q + contract(fq, direction[:, :width_q], 1, 0)
        step_all_o = step_all_o + contract(fo, direction[:, width_q:], 1, 0)
    q = jnp.concatenate([held_q[0].reshape(-1, LANES), held_q[1].reshape(-1, LANES)[:, : width_q - LANES]], axis=1)
    copy_q_t[...] = (q - 0.02 * (step_all_q * scale_q)).T.astype(BF16)
    o = jnp.concatenate([held_o[0].reshape(-1, LANES), held_o[1].reshape(-1, LANES)], axis=1)
    copy_o[...] = (o - 0.02 * (step_all_o * scale_o)).astype(BF16)


def on_device(
    latent_in,
    query_cot,
    attn_out,
    mix_cot,
    query_weight,
    output_weight,
    query_factor,
    output_factor,
    query_mean,
    query_square,
    output_mean,
    output_square,
):
    count = lax.axis_size("fs")
    columns = lax.axis_size("tp")
    inv_root = 1.0 / math.sqrt(latent_in.shape[0] * count)
    rows_q, width_q = query_weight.shape
    rows_o, width_o = output_weight.shape
    rank = query_factor.shape[1]
    width = width_q + width_o
    rows = rows_q + rows_o
    quarter = 24

    (packed,) = on_chip(
        pack_body,
        [((count, rows + quarter, LANES), BF16)],
        query_factor, output_factor, query_weight, output_weight,
    )
    own = exchange(packed, "fs")
    grad_q_t = contract(query_cot, latent_in, 0, 0).astype(BF16)
    grad_o = contract(attn_out, mix_cot, 0, 0).astype(BF16)
    other = lax.ppermute(own, "tp", [(i, i ^ 1) for i in range(columns)])
    held = [own[:, rows:]]
    for k in range(1, RING):
        pairs = [(i, i // RING * RING + (i + k) % RING) for i in range(count)]
        held.append(lax.ppermute(held[0], "fs", pairs))

    (low,) = on_chip(
        functools.partial(low_body, inv_root, rows_q, rows),
        [((count, rank // count, width), BF16)],
        own, other, grad_q_t, grad_o,
    )
    parts = exchange(low, "fs")
    of_q = (query_mean.shape, F32)
    of_o = (output_mean.shape, F32)
    mean_q, square_q, mean_o, square_o, joined = on_chip(
        moments_body,
        [of_q, of_q, of_o, of_o, ((count, rank // count, width), BF16)],
        parts, query_mean, query_square, output_mean, output_square,
    )
    piece = exchange(joined, "fs")
    (sums,) = on_chip(functools.partial(sums_body, width_q), [((columns, 8, LANES), F32)], piece)
    sums = exchange(sums, "tp")
    sizes = (rank * width_q * columns, rank * width_o * columns)
    step_q, step_o, new_q, new_o, copy_q_t, copy_o = on_chip(
        functools.partial(final_body, sizes),
        [
            ((rows_q, width_q), F32),
            ((rows_o, width_o), F32),
            ((rows_q, width_q), F32),
            ((rows_o, width_o), F32),
            ((width_q, rows_q * count), BF16),
            ((rows_o * count, width_o), BF16),
        ],
        own, other, *held, piece, sums, query_factor, output_factor, query_weight, output_weight,
        scratch=(
            pltpu.VMEM((2, count, 2, 8, LANES), F32),
            pltpu.VMEM((2, count, RING, 8, LANES), F32),
        ),
    )
    return (step_q, step_o, new_q, new_o, copy_q_t.T, copy_o, mean_q, square_q, mean_o, square_o)


def solution(mesh):
    rows = P("fs", None)
    both = P("fs", "tp")
    gathered = P(None, "tp")
    return jax.shard_map(
        on_device,
        mesh=mesh,
        in_specs=(rows, both, rows, both, both, both, rows, rows, both, both, both, both),
        out_specs=(both, both, both, both, gathered, gathered, both, both, both, both),
        check_vma=False,
    )
```

time: 137 us -> 95.7 us (0.70)
  the two profiles are of different devices: /device:TPU:2 before, /device:TPU:1 now
where the time goes in v2:
time: 95.7 us; the launch traced here: 95.2 us
  starting transfers between devices  30 us (31%)
  waiting for transfers between devices  24.9 us (26%)
  blocking collectives  16.6 us (17%)
  Pallas kernels  11.5 us (12%)
  matrix products  8.59 us (9%)
  local copies, waits for them, and re-layouts  2.96 us (3%)
    all_to_all x3, waiting for transfers between devices, exchange(): return lax.all_to_all(tiles, axis, split_axis=0, concat_axis=0, tiled=True)  24.9 us
    all_to_all x3, starting transfers between devices, exchange(): return lax.all_to_all(tiles, axis, split_axis=0, concat_axis=0, tiled=True)  24 us
    all_to_all x1, blocking collectives, exchange(): return lax.all_to_all(tiles, axis, split_axis=0, concat_axis=0, tiled=True)  16.6 us
    pallas_call x5, Pallas kernels, on_chip(): pl.pallas_call(body, out_shape=tuple((jax.ShapeDtypeStruct(s, d) for s, d...  11.5 us
    dot_general x2, matrix products, contract(): return lax.dot_general(left, right, dims, preferred_element_type=F32)  8.59 us
    ppermute x3, starting transfers between devices, on_device(): held.append(lax.ppermute(held[0], 'fs', pairs))  3.59 us
    ppermute x1, starting transfers between devices, on_device(): other = lax.ppermute(own, 'tp', [(i, i ^ 1) for i in range(columns)])  2.38 us
  transfers between devices with their start and end apart: 7, of which 3 were waited for; matrix products, arithmetic and copies ran while one was open for 11% of the time, Pallas kernels for 2%

profile of v2, /device:TPU:1, one launch (start us, length us, event | category | flops | bytes accessed | tf_op | source)
XLA Modules:
  0.0 95.2 jit_solution(3892664429911957704)
XLA Ops:
  0.6 0.0 copy-start
  0.7 1.8 %shard_map.195 = bf16[32,72,128]{2,1,0:T(8,128)(2,1)} custom-call(bf16[16,256]{1,0:T(8,128)(2,1)} %fq_own.1, bf16[32,256]{1,0:T(8,128)(2,1)} %fo_own.1, f32[16,192]{1,0:T(8,128)} %wq.3, f32[32,256]{1,0:T(8,128)} %wo.3), custom_call_target="tpu_custom_call" | custom-call | tf_op jit(solution)/shard_map/pallas_call | solution.py:28
  2.5 12.1 %all-to-all-start = ((bf16[32,72,128]{2,1,0:T(8,128)(2,1)}), bf16[32,72,128]{2,1,0:T(8,128)(2,1)}, u32[]{:S(2)}, u32[]{:S(2)}) async-start(bf16[32,72,128]{2,1,0:T(8,128)(2,1)} %shard_map.195), calls=%async_computation | async-start | bytes 1179648 | tf_op jit(solution)/shard_map/all_to_all | solution.py:18
  14.6 0.0 copy-done
  14.7 2.7 %convolution_convert_fusion.1.gq_t = bf16[192,512]{1,0:T(8,128)(2,1)} fusion(bf16[3072,192]{0,1:T(8,128)(2,1)} %param.13, bf16[3072,512]{1,0:T(8,128)(2,1)S(1)} %copy-done), kind=kOutput, calls=%fused_computation.1 | convolution fusion | flops 604078080 | bytes 4521984 | tf_op jit(solution)/shard_map/dot_general | solution.py:23
  17.4 14.8 %all-to-all-done.own = bf16[32,72,128]{2,1,0:T(8,128)(2,1)} async-done(((bf16[32,72,128]{2,1,0:T(8,128)(2,1)}), bf16[32,72,128]{2,1,0:T(8,128)(2,1)}, u32[]{:S(2)}, u32[]{:S(2)}) %all-to-all-start) | async-done | bytes 589856 | tf_op jit(solution)/shard_map/all_to_all | solution.py:18
  32.2 2.4 %collective-permute-start = (bf16[32,72,128]{2,1,0:T(8,128)(2,1)}, bf16[32,72,128]{2,1,0:T(8,128)(2,1)}, u32[]{:S(2)}, u32[]{:S(2)}) collective-permute-start(bf16[32,72,128]{2,1,0:T(8,128)(2,1)} %all-to-all-done.own), channel_id=1, source_target_pairs={{0,1},{1,0},{2,3},{3,2},{4,5},{5,4},{6,7},{7,6},{8,9},{9,8},{10,11... | collective-permute-start | bytes 1769480 | tf_op jit(solution)/shard_map/ppermute | solution.py:175
  34.6 5.9 %convolution_convert_fusion.go = bf16[1024,256]{1,0:T(8,128)(2,1)} fusion(bf16[3072,1024]{1,0:T(8,128)(2,1)} %param.14, bf16[3072,256]{1,0:T(8,128)(2,1)} %param.15), kind=kOutput, calls=%fused_computation | convolution fusion | flops 1610874880 | bytes 8388608 | tf_op jit(solution)/shard_map/dot_general | solution.py:23
  40.4 0.0 collective-permute-done.other
  40.4 2.6 %shard_map.196 = bf16[32,8,448]{2,1,0:T(8,128)(2,1)} custom-call(bf16[32,72,128]{2,1,0:T(8,128)(2,1)} %all-to-all-done.own, bf16[32,72,128]{2,1,0:T(8,128)(2,1)} %collective-permute-done.other, bf16[192,512]{1,0:T(8,128)(2,1)} %convolution_convert_fusion.1.gq_t, bf16[1024,256]{1,0:T(8,128)(2,1)} %convolution_convert_fusion.go), custom_call_target="tpu_custom_call" | custom-call | tf_op jit(solution)/shard_map/pallas_call | solution.py:28
  43.1 16.6 %all_to_all.20.parts = bf16[32,8,448]{2,1,0:T(8,128)(2,1)} all-to-all(bf16[32,8,448]{2,1,0:T(8,128)(2,1)} %shard_map.196), channel_id=1, replica_groups=mesh['fs'=32,'tp'=8] {'fs'}, dimensions={0} | all-to-all | bytes 458752 | tf_op jit(solution)/shard_map/all_to_all | solution.py:18
  59.7 1.9 %shard_map.197 = (f32[8,192]{1,0:T(8,128)}, f32[8,192]{1,0:T(8,128)}, f32[8,256]{1,0:T(8,128)}, f32[8,256]{1,0:T(8,128)}, bf16[32,8,448]{2,1,0:T(8,128)(2,1)}) custom-call(bf16[32,8,448]{2,1,0:T(8,128)(2,1)} %all_to_all.20.parts, f32[8,192]{1,0:T(8,128)} %mq.1, f32[8,192]{1,0:T(8,128)} %sq.1, f32[8,256]{1,0:T(8,128)} %mo.1, f32[8,256]{1,0:T(8,128)} %so.1), custom_call_target="tpu_custom_call" | custom-call | tf_op jit(solution)/shard_map/pallas_call | solution.py:28
  61.6 4.2 %all-to-all-start.2 = ((bf16[32,8,448]{2,1,0:T(8,128)(2,1)}), bf16[32,8,448]{2,1,0:T(8,128)(2,1)S(1)}, u32[]{:S(2)}, u32[]{:S(2)}) async-start(bf16[32,8,448]{2,1,0:T(8,128)(2,1)} %get-tuple-element.21), calls=%async_computation.2 | async-start | bytes 524288 | tf_op jit(solution)/shard_map/all_to_all | solution.py:18
  65.8 1.6 %slice.4.w0 = bf16[32,24,128]{2,1,0:T(8,128)(2,1)} slice(bf16[32,72,128]{2,1,0:T(8,128)(2,1)} %all-to-all-done.own), slice={[0:32], [48:72], [0:128]} | slice | bytes 393216 | tf_op jit(solution)/shard_map/slice | solution.py:176
  67.5 2.4 %collective-permute-start.3 = (bf16[32,24,128]{2,1,0:T(8,128)(2,1)}, bf16[32,24,128]{2,1,0:T(8,128)(2,1)}, u32[]{:S(2)}, u32[]{:S(2)}) collective-permute-start(bf16[32,24,128]{2,1,0:T(8,128)(2,1)} %slice.4.w0), channel_id=1, source_target_pairs={{0,24},{8,0},{16,8},{24,16},{32,56},{40,32},{48,40},{56,48},{64,88... | collective-permute-start | bytes 589832 | tf_op jit(solution)/shard_map/ppermute | solution.py:179
  69.9 0.6 collective-permute-start.2
  70.5 0.6 collective-permute-start.1
  71.1 5.3 %all-to-all-done.2.piece = bf16[32,8,448]{2,1,0:T(8,128)(2,1)S(1)} async-done(((bf16[32,8,448]{2,1,0:T(8,128)(2,1)}), bf16[32,8,448]{2,1,0:T(8,128)(2,1)S(1)}, u32[]{:S(2)}, u32[]{:S(2)}) %all-to-all-start.2) | async-done | bytes 229408 | tf_op jit(solution)/shard_map/all_to_all | solution.py:18
  76.4 0.0 copy-start.1
  76.4 0.7 copy-done.1
  77.1 1.8 %shard_map.198 = f32[8,8,128]{2,1,0:T(8,128)} custom-call(bf16[32,8,448]{2,1,0:T(8,128)(2,1)} %copy-done.1), custom_call_target="tpu_custom_call" | custom-call | tf_op jit(solution)/shard_map/pallas_call | solution.py:28
  78.9 7.7 %all-to-all-start.3 = ((f32[8,8,128]{2,1,0:T(8,128)}), f32[8,8,128]{2,1,0:T(8,128)S(1)}, u32[]{:S(2)}, u32[]{:S(2)}) async-start(f32[8,8,128]{2,1,0:T(8,128)} %shard_map.198), calls=%async_computation.3 | async-start | bytes 65536 | tf_op jit(solution)/shard_map/all_to_all | solution.py:18
  86.6 0.0 collective-permute-done.3.w3
  86.6 0.0 collective-permute-done.2.w2
  86.6 0.0 collective-permute-done.1.w1
  86.6 4.7 %all-to-all-done.3.sums = f32[8,8,128]{2,1,0:T(8,128)S(1)} async-done(((f32[8,8,128]{2,1,0:T(8,128)}), f32[8,8,128]{2,1,0:T(8,128)S(1)}, u32[]{:S(2)}, u32[]{:S(2)}) %all-to-all-start.3) | async-done | bytes 32800 | tf_op jit(solution)/shard_map/all_to_all | solution.py:18
  91.3 0.0 copy-start.2
  91.3 0.6 copy-done.2
  91.9 3.3 %shard_map.199 = (f32[16,192]{1,0:T(8,128)}, f32[32,256]{1,0:T(8,128)}, f32[16,192]{1,0:T(8,128)}, f32[32,256]{1,0:T(8,128)}, bf16[192,512]{1,0:T(8,128)(2,1)}, /*index=5*/bf16[1024,256]{1,0:T(8,128)(2,1)}) custom-call(bf16[32,72,128]{2,1,0:T(8,128)(2,1)} %all-to-all-done.own, bf16[32,72,128]{2,1,0:T(8,128)(2,1)} %collective-permute-done.other, ...), custom_call_target="tpu_custom_call" | custom-call | tf_op jit(solution)/shard_map/pallas_call | solution.py:28
Async XLA Ops:
  0.6 14.0 %copy-start = (bf16[3072,512]{1,0:T(8,128)(2,1)S(1)}, bf16[3072,512]{1,0:T(8,128)(2,1)}, u32[]{:S(2)}) copy-start(bf16[3072,512]{1,0:T(8,128)(2,1)} %param.12) | copy-start | bytes 9437188
  2.5 29.7 %all-to-all-start = ((bf16[32,72,128]{2,1,0:T(8,128)(2,1)}), bf16[32,72,128]{2,1,0:T(8,128)(2,1)}, u32[]{:S(2)}, u32[]{:S(2)}) async-start(bf16[32,72,128]{2,1,0:T(8,128)(2,1)} %shard_map.195), calls=%async_computation | async-start | bytes 1179648 | tf_op jit(solution)/shard_map/all_to_all | solution.py:18
  32.2 8.2 %collective-permute-start = (bf16[32,72,128]{2,1,0:T(8,128)(2,1)}, bf16[32,72,128]{2,1,0:T(8,128)(2,1)}, u32[]{:S(2)}, u32[]{:S(2)}) collective-permute-start(bf16[32,72,128]{2,1,0:T(8,128)(2,1)} %all-to-all-done.own), channel_id=1, source_target_pairs={{0,1},{1,0},{2,3},{3,2},{4,5},{5,4},{6,7},{7,6},{8,9},{9,8},{10,11... | collective-permute-start | bytes 1769480 | tf_op jit(solution)/shard_map/ppermute | solution.py:175
  61.6 14.8 %all-to-all-start.2 = ((bf16[32,8,448]{2,1,0:T(8,128)(2,1)}), bf16[32,8,448]{2,1,0:T(8,128)(2,1)S(1)}, u32[]{:S(2)}, u32[]{:S(2)}) async-start(bf16[32,8,448]{2,1,0:T(8,128)(2,1)} %get-tuple-element.21), calls=%async_computation.2 | async-start | bytes 524288 | tf_op jit(solution)/shard_map/all_to_all | solution.py:18
  67.5 19.1 %collective-permute-start.3 = (bf16[32,24,128]{2,1,0:T(8,128)(2,1)}, bf16[32,24,128]{2,1,0:T(8,128)(2,1)}, u32[]{:S(2)}, u32[]{:S(2)}) collective-permute-start(bf16[32,24,128]{2,1,0:T(8,128)(2,1)} %slice.4.w0), channel_id=1, source_target_pairs={{0,24},{8,0},{16,8},{24,16},{32,56},{40,32},{48,40},{56,48},{64,88... | collective-permute-start | bytes 589832 | tf_op jit(solution)/shard_map/ppermute | solution.py:179
  69.9 16.7 %collective-permute-start.2 = (bf16[32,24,128]{2,1,0:T(8,128)(2,1)}, bf16[32,24,128]{2,1,0:T(8,128)(2,1)}, u32[]{:S(2)}, u32[]{:S(2)}) collective-permute-start(bf16[32,24,128]{2,1,0:T(8,128)(2,1)} %slice.4.w0), channel_id=1, source_target_pairs={{0,16},{8,24},{16,0},{24,8},{32,48},{40,56},{48,32},{56,40},{64,80... | collective-permute-start | bytes 589832 | tf_op jit(solution)/shard_map/ppermute | solution.py:179
  70.5 16.1 %collective-permute-start.1 = (bf16[32,24,128]{2,1,0:T(8,128)(2,1)}, bf16[32,24,128]{2,1,0:T(8,128)(2,1)}, u32[]{:S(2)}, u32[]{:S(2)}) collective-permute-start(bf16[32,24,128]{2,1,0:T(8,128)(2,1)} %slice.4.w0), channel_id=1, source_target_pairs={{0,8},{8,16},{16,24},{24,0},{32,40},{40,48},{48,56},{56,32},{64,72... | collective-permute-start | bytes 589832 | tf_op jit(solution)/shard_map/ppermute | solution.py:179
  76.4 0.7 copy-start.1
  78.9 12.4 %all-to-all-start.3 = ((f32[8,8,128]{2,1,0:T(8,128)}), f32[8,8,128]{2,1,0:T(8,128)S(1)}, u32[]{:S(2)}, u32[]{:S(2)}) async-start(f32[8,8,128]{2,1,0:T(8,128)} %shard_map.198), calls=%async_computation.3 | async-start | bytes 65536 | tf_op jit(solution)/shard_map/all_to_all | solution.py:18
  91.3 0.6 copy-start.2

commit v3 on v2

--- a/solution.py
+++ b/solution.py
@@ -11,6 +11,7 @@
 BF16 = jnp.bfloat16
 F32 = jnp.float32
 LANES = 128
+SMALL = 16 * 2**20
 RING = 4
 
 
@@ -23,14 +24,19 @@
     return lax.dot_general(left, right, dims, preferred_element_type=F32)
 
 
-def on_chip(body, outs, *args, scratch=()):
+def near(x):
+    return pltpu.with_memory_space_constraint(x, pltpu.VMEM)
+
+
+def on_chip(body, outs, *args, scratch=(), limit=None, copied=False):
     vmem = pl.BlockSpec(memory_space=pltpu.VMEM)
     return pl.pallas_call(
         body,
-        out_shape=tuple(jax.ShapeDtypeStruct(s, d) for s, d in outs),
+        out_shape=tuple(pltpu.VMEM(s, d) if stays else jax.ShapeDtypeStruct(s, d) for s, d, stays in outs),
         in_specs=[vmem] * len(args),
-        out_specs=tuple(vmem for _ in outs),
+        out_specs=tuple(pl.BlockSpec(memory_space=pl.ANY) if copied else vmem for _ in outs),
         scratch_shapes=list(scratch),
+        compiler_params=pltpu.CompilerParams(vmem_limit_bytes=limit),
     )(*args)
 
 
@@ -38,25 +44,31 @@
     return x[:, :LANES], x[:, LANES:]
 
 
-def pack_body(fq, fo, wq, wo, out):
+def pack_body(fq, fo, wq, wo, out, tiles, sems):
     count = out.shape[0]
     core = lax.axis_index("tp") % 2
     rows_q, rows_o = fq.shape[0], fo.shape[0]
     rows = rows_q + rows_o
-    for f, at in ((fq, 0), (fo, rows_q)):
-        left, right = halves(f[...])
-        half = jnp.where(core == 0, left.astype(F32), right.astype(F32)).astype(BF16)
-        out[:, at : at + f.shape[0]] = jnp.broadcast_to(half, (count, *half.shape))
     width_q = wq.shape[1]
     for y in range(RING):
+        for f, at in ((fq, 0), (fo, rows_q)):
+            left, right = halves(f[...])
+            half = jnp.where(core == 0, left.astype(F32), right.astype(F32)).astype(BF16)
+            tiles[y, at : at + f.shape[0]] = half
         row, col = y % 2, y // 2
         part = wq[8 * row : 8 * row + 8, col * LANES : min(width_q, (col + 1) * LANES)]
         if part.shape[1] < LANES:
             part = jnp.concatenate([part, jnp.zeros((8, LANES - part.shape[1]), F32)], axis=1)
         left, right = halves(wo[8 * y : 8 * y + 8, :])
-        quarter = jnp.concatenate([part, left, right], axis=0).astype(BF16)
-        for z in range(count // RING):
-            out[z * RING + y, rows:] = quarter
+        tiles[y, rows:] = jnp.concatenate([part, left, right], axis=0).astype(BF16)
+    copies = [
+        pltpu.make_async_copy(tiles, out.at[pl.ds(z * RING, RING)], sems.at[z])
+        for z in range(count // RING)
+    ]
+    for copy in copies:
+        copy.start()
+    for copy in copies:
+        copy.wait()
 
 
 def low_body(inv_root, rows_q, rows, own, other, gq_t, go, out):
@@ -98,34 +110,15 @@
     out[:, half[1] :] = jnp.broadcast_to(jnp.sum(squares[:, width_q:], keepdims=True)[None], half)
 
 
-def final_body(
-    sizes, own, other, w0, w1, w2, w3, piece, sums, fq_own, fo_own, wq, wo,
-    step_q, step_o, new_q, new_o, copy_q_t, copy_o, held_q, held_o,
-):
+def product_body(own, other, piece, fq_own, fo_own, step_q, step_o, all_q, all_o):
     core = lax.axis_index("tp") % 2
-    y = lax.axis_index("fs") % RING
-    rows_q, width_q = wq.shape
-    rows = rows_q + wo.shape[0]
+    rows_q, width_q = step_q.shape
+    rows = rows_q + step_o.shape[0]
     count = own.shape[0]
-    for k, ref in enumerate((w0, w1, w2, w3)):
-        u = (y + (RING - k)) % RING
-        got = ref[...].astype(F32)
-        held_q[u // 2, :, u % 2] = got[:, 0:8]
-        held_o[0, :, u] = got[:, 8:16]
-        held_o[1, :, u] = got[:, 16:24]
-    total = jnp.sum(sums[...], axis=0)
-    middle = total.shape[0] // 2
-    scale_q = 1.0 / jnp.sqrt(total[0:1, :1] / sizes[0] + 0.25)
-    scale_o = 1.0 / jnp.sqrt(total[middle : middle + 1, :1] / sizes[1] + 0.25)
     rank = fq_own.shape[1]
     whole = piece[...].reshape(rank, -1)
-    for f, w, step, new, scale, direction in (
-        (fq_own, wq, step_q, new_q, scale_q, whole[:, :width_q]),
-        (fo_own, wo, step_o, new_o, scale_o, whole[:, width_q:]),
-    ):
-        step_own = contract(f[...], direction, 1, 0) * scale
-        step[...] = step_own
-        new[...] = w[...] - 0.02 * step_own
+    step_q[...] = contract(fq_own[...], whole[:, :width_q], 1, 0)
+    step_o[...] = contract(fo_own[...], whole[:, width_q:], 1, 0)
     step_all_q = 0.0
     step_all_o = 0.0
     for ref, at in ((own, core), (other, 1 - core)):
@@ -134,10 +127,43 @@
         fo = ref[:, rows_q:rows].reshape(count * (rows - rows_q), LANES)
         step_all_q = step_all_q + contract(fq, direction[:, :width_q], 1, 0)
         step_all_o = step_all_o + contract(fo, direction[:, width_q:], 1, 0)
-    q = jnp.concatenate([held_q[0].reshape(-1, LANES), held_q[1].reshape(-1, LANES)[:, : width_q - LANES]], axis=1)
-    copy_q_t[...] = (q - 0.02 * (step_all_q * scale_q)).T.astype(BF16)
-    o = jnp.concatenate([held_o[0].reshape(-1, LANES), held_o[1].reshape(-1, LANES)], axis=1)
-    copy_o[...] = (o - 0.02 * (step_all_o * scale_o)).astype(BF16)
+    all_q[...] = step_all_q.T.astype(BF16)
+    all_o[...] = step_all_o.astype(BF16)
+
+
+def assemble_body(w0, w1, w2, w3, whole_q_t, whole_o, held_q, held_o):
+    y = lax.axis_index("fs") % RING
+    width_q = whole_q_t.shape[0]
+    for k, ref in enumerate((w0, w1, w2, w3)):
+        u = (y + (RING - k)) % RING
+        got = ref[...].astype(F32)
+        held_q[u // 2, :, u % 2] = got[:, 0:8]
+        held_o[0, :, u] = got[:, 8:16]
+        held_o[1, :, u] = got[:, 16:24]
+    for part in range(2):
+        at = slice(part * LANES, min(width_q, (part + 1) * LANES))
+        whole_q_t[at] = held_q[part].reshape(-1, LANES).T[: at.stop - at.start].astype(BF16)
+        at = slice(part * LANES, (part + 1) * LANES)
+        whole_o[:, at] = held_o[part].reshape(-1, LANES).astype(BF16)
+
+
+def final_body(
+    sizes, whole_q_t, whole_o, sums, pq_own, po_own, pq_all, po_all, wq, wo,
+    step_q, step_o, new_q, new_o, copy_q_t, copy_o,
+):
+    total = jnp.sum(sums[...], axis=0)
+    middle = total.shape[0] // 2
+    scale_q = 1.0 / jnp.sqrt(total[0:1, :1] / sizes[0] + 0.25)
+    scale_o = 1.0 / jnp.sqrt(total[middle : middle + 1, :1] / sizes[1] + 0.25)
+    for p, w, step, new, scale in (
+        (pq_own, wq, step_q, new_q, scale_q),
+        (po_own, wo, step_o, new_o, scale_o),
+    ):
+        step_own = p[...] * scale
+        step[...] = step_own
+        new[...] = w[...] - 0.02 * step_own
+    for w, p, copy, scale in ((whole_q_t, pq_all, copy_q_t, scale_q), (whole_o, po_all, copy_o, scale_o)):
+        copy[...] = (w[...].astype(F32) - 0.02 * (p[...].astype(F32) * scale)).astype(BF16)
 
 
 def on_device(
@@ -166,8 +192,13 @@
 
     (packed,) = on_chip(
         pack_body,
-        [((count, rows + quarter, LANES), BF16)],
+        [((count, rows + quarter, LANES), BF16, False)],
         query_factor, output_factor, query_weight, output_weight,
+        scratch=(
+            pltpu.VMEM((RING, rows + quarter, LANES), BF16),
+            pltpu.SemaphoreType.DMA((count // RING,)),
+        ),
+        copied=True,
     )
     own = exchange(packed, "fs")
     grad_q_t = contract(query_cot, latent_in, 0, 0).astype(BF16)
@@ -180,36 +211,53 @@
 
     (low,) = on_chip(
         functools.partial(low_body, inv_root, rows_q, rows),
-        [((count, rank // count, width), BF16)],
-        own, other, grad_q_t, grad_o,
+        [((count, rank // count, width), BF16, True)],
+        own, other, near(grad_q_t), near(grad_o),
     )
     parts = exchange(low, "fs")
-    of_q = (query_mean.shape, F32)
-    of_o = (output_mean.shape, F32)
+    of_q = (query_mean.shape, F32, False)
+    of_o = (output_mean.shape, F32, False)
     mean_q, square_q, mean_o, square_o, joined = on_chip(
         moments_body,
-        [of_q, of_q, of_o, of_o, ((count, rank // count, width), BF16)],
-        parts, query_mean, query_square, output_mean, output_square,
+        [of_q, of_q, of_o, of_o, ((count, rank // count, width), BF16, False)],
+        near(parts), query_mean, query_square, output_mean, output_square, limit=SMALL,
     )
     piece = exchange(joined, "fs")
-    (sums,) = on_chip(functools.partial(sums_body, width_q), [((columns, 8, LANES), F32)], piece)
-    sums = exchange(sums, "tp")
-    sizes = (rank * width_q * columns, rank * width_o * columns)
-    step_q, step_o, new_q, new_o, copy_q_t, copy_o = on_chip(
-        functools.partial(final_body, sizes),
-        [
-            ((rows_q, width_q), F32),
-            ((rows_o, width_o), F32),
-            ((rows_q, width_q), F32),
-            ((rows_o, width_o), F32),
-            ((width_q, rows_q * count), BF16),
-            ((rows_o * count, width_o), BF16),
-        ],
-        own, other, *held, piece, sums, query_factor, output_factor, query_weight, output_weight,
+    wholes = on_chip(
+        assemble_body,
+        [((width_q, rows_q * count), BF16, False), ((rows_o * count, width_o), BF16, False)],
+        *held,
         scratch=(
             pltpu.VMEM((2, count, 2, 8, LANES), F32),
             pltpu.VMEM((2, count, RING, 8, LANES), F32),
         ),
+    )
+    (sums,) = on_chip(
+        functools.partial(sums_body, width_q), [((columns, 8, LANES), F32, False)], near(piece), limit=SMALL
+    )
+    sums = exchange(sums, "tp")
+    sizes = (rank * width_q * columns, rank * width_o * columns)
+    products = on_chip(
+        product_body,
+        [
+            ((rows_q, width_q), F32, True),
+            ((rows_o, width_o), F32, True),
+            ((width_q, rows_q * count), BF16, True),
+            ((rows_o * count, width_o), BF16, True),
+        ],
+        own, other, near(piece), query_factor, output_factor,
+    )
+    step_q, step_o, new_q, new_o, copy_q_t, copy_o = on_chip(
+        functools.partial(final_body, sizes),
+        [
+            ((rows_q, width_q), F32, False),
+            ((rows_o, width_o), F32, False),
+            ((rows_q, width_q), F32, False),
+            ((rows_o, width_o), F32, False),
+            ((width_q, rows_q * count), BF16, False),
+            ((rows_o * count, width_o), BF16, False),
+        ],
+        *wholes, near(sums), *map(near, products), query_weight, output_weight,
     )
     return (step_q, step_o, new_q, new_o, copy_q_t.T, copy_o, mean_q, square_q, mean_o, square_o)
 

time: 95.7 us -> 91 us (0.951)
  the two profiles are of different devices: /device:TPU:1 before, /device:TPU:2 now
where the time goes in v3:
time: 91 us; the launch traced here: 89.5 us
  starting transfers between devices  24.9 us (27%)
  waiting for transfers between devices  22.6 us (25%)
  blocking collectives  18.1 us (20%)
  Pallas kernels  12 us (13%)
  matrix products  7.86 us (9%)
  local copies, waits for them, and re-layouts  3.2 us (4%)
    all_to_all x3, waiting for transfers between devices, exchange(): return lax.all_to_all(tiles, axis, split_axis=0, concat_axis=0, tiled=True)  22.5 us
    all_to_all x3, starting transfers between devices, exchange(): return lax.all_to_all(tiles, axis, split_axis=0, concat_axis=0, tiled=True)  20.2 us
    all_to_all x1, blocking collectives, exchange(): return lax.all_to_all(tiles, axis, split_axis=0, concat_axis=0, tiled=True)  18.1 us
    pallas_call x7, Pallas kernels, on_chip(): pl.pallas_call(body, out_shape=tuple((pltpu.VMEM(s, d) if stays else jax....  12 us
    dot_general x2, matrix products, contract(): return lax.dot_general(left, right, dims, preferred_element_type=F32)  7.86 us
    ppermute x3, starting transfers between devices, on_device(): held.append(lax.ppermute(held[0], 'fs', pairs))  4.69 us
    unnamed x22, local copies, waits for them, and re-layouts  2.25 us
  transfers between devices with their start and end apart: 7, of which 2 were waited for; matrix products, arithmetic and copies ran while one was open for 10% of the time, Pallas kernels for 6%

profile of v3, /device:TPU:2, one launch (start us, length us, event | category | flops | bytes accessed | tf_op | source)
XLA Modules:
  0.0 89.5 jit_solution(11779106524739524129)
XLA Ops:
  0.6 0.0 copy-start
  0.7 1.8 %shard_map.195 = bf16[32,72,128]{2,1,0:T(8,128)(2,1)} custom-call(bf16[16,256]{1,0:T(8,128)(2,1)} %fq_own.1, bf16[32,256]{1,0:T(8,128)(2,1)} %fo_own.1, f32[16,192]{1,0:T(8,128)} %wq.3, f32[32,256]{1,0:T(8,128)} %wo.3), custom_call_target="tpu_custom_call" | custom-call | tf_op jit(solution)/shard_map/pallas_call | solution.py:33
  2.5 11.5 %all-to-all-start = ((bf16[32,72,128]{2,1,0:T(8,128)(2,1)}), bf16[32,72,128]{2,1,0:T(8,128)(2,1)S(1)}, u32[]{:S(2)}, u32[]{:S(2)}) async-start(bf16[32,72,128]{2,1,0:T(8,128)(2,1)} %shard_map.195), calls=%async_computation | async-start | bytes 1179648 | tf_op jit(solution)/shard_map/all_to_all | solution.py:19
  14.0 3.0 %convolution_convert_fusion.1.gq_t = bf16[192,512]{1,0:T(8,128)(2,1)S(1)} fusion(bf16[3072,192]{0,1:T(8,128)(2,1)} %param.13, bf16[3072,512]{1,0:T(8,128)(2,1)} %param.12), kind=kOutput, calls=%fused_computation.1 | convolution fusion | flops 604078080 | bytes 4521984 | tf_op jit(solution)/shard_map/dot_general | solution.py:24
  17.0 0.0 copy-start.1
  17.1 0.0 copy-start.2
  17.1 0.0 copy-start.3
  17.1 0.0 copy-start.4
  17.1 15.9 %all-to-all-done.own = bf16[32,72,128]{2,1,0:T(8,128)(2,1)S(1)} async-done(((bf16[32,72,128]{2,1,0:T(8,128)(2,1)}), bf16[32,72,128]{2,1,0:T(8,128)(2,1)S(1)}, u32[]{:S(2)}, u32[]{:S(2)}) %all-to-all-start) | async-done | bytes 589856 | tf_op jit(solution)/shard_map/all_to_all | solution.py:19
  33.0 0.0 collective-permute-start.3
  33.0 4.8 %convolution_convert_fusion.go = bf16[1024,256]{1,0:T(8,128)(2,1)S(1)} fusion(bf16[3072,1024]{1,0:T(8,128)(2,1)} %param.14, bf16[3072,256]{1,0:T(8,128)(2,1)S(1)} %copy-done), kind=kOutput, calls=%fused_computation | convolution fusion | flops 1610874880 | bytes 8388608 | tf_op jit(solution)/shard_map/dot_general | solution.py:24
  37.9 0.0 collective-permute-done.3.other
  37.9 0.8 copy-done.6
  38.7 1.7 %shard_map.197 = bf16[32,8,448]{2,1,0:T(8,128)(2,1)S(1)} custom-call(bf16[32,72,128]{2,1,0:T(8,128)(2,1)} %copy-done.5, bf16[32,72,128]{2,1,0:T(8,128)(2,1)} %copy-done.6, bf16[192,512]{1,0:T(8,128)(2,1)S(1)} %convolution_convert_fusion.1.gq_t, bf16[1024,256]{1,0:T(8,128)(2,1)S(1)} %convolution_convert_fusion.go), custom_call_target="tpu_custom_call" | custom-call | tf_op jit(solution)/shard_map/pallas_call | solution.py:33
  40.4 18.1 %all_to_all.20.parts = bf16[32,8,448]{2,1,0:T(8,128)(2,1)S(1)} all-to-all(bf16[32,8,448]{2,1,0:T(8,128)(2,1)S(1)} %shard_map.197), channel_id=1, replica_groups=mesh['fs'=32,'tp'=8] {'fs'}, dimensions={0} | all-to-all | bytes 458752 | tf_op jit(solution)/shard_map/all_to_all | solution.py:19
  58.6 0.9 %shard_map.198 = (f32[8,192]{1,0:T(8,128)}, f32[8,192]{1,0:T(8,128)}, f32[8,256]{1,0:T(8,128)}, f32[8,256]{1,0:T(8,128)}, bf16[32,8,448]{2,1,0:T(8,128)(2,1)}) custom-call(bf16[32,8,448]{2,1,0:T(8,128)(2,1)S(1)} %all_to_all.20.parts, f32[8,192]{1,0:T(8,128)S(1)} %copy-done.1, f32[8,192]{1,0:T(8,128)S(1)} %copy-done.2, f32[8,256]{1,0:T(8,128)S(1)} %copy-done.3, ...), custom_call_target="tpu_custom_call" | custom-call | tf_op jit(solution)/shard_map/pallas_call | solution.py:33
  59.5 3.9 %all-to-all-start.2 = ((bf16[32,8,448]{2,1,0:T(8,128)(2,1)}), bf16[32,8,448]{2,1,0:T(8,128)(2,1)S(1)}, u32[]{:S(2)}, u32[]{:S(2)}) async-start(bf16[32,8,448]{2,1,0:T(8,128)(2,1)} %get-tuple-element.29), calls=%async_computation.2 | async-start | bytes 524288 | tf_op jit(solution)/shard_map/all_to_all | solution.py:19
  63.4 1.0 %slice.4.w0 = bf16[32,24,128]{2,1,0:T(8,128)(2,1)S(1)} slice(bf16[32,72,128]{2,1,0:T(8,128)(2,1)} %copy-done.5), slice={[0:32], [48:72], [0:128]} | slice | bytes 393216 | tf_op jit(solution)/shard_map/slice | solution.py:207
  64.3 0.0 copy-start.7
  64.3 3.0 %collective-permute-start.2 = (bf16[32,24,128]{2,1,0:T(8,128)(2,1)S(1)}, bf16[32,24,128]{2,1,0:T(8,128)(2,1)S(1)}, u32[]{:S(2)}, u32[]{:S(2)}) collective-permute-start(bf16[32,24,128]{2,1,0:T(8,128)(2,1)S(1)} %slice.4.w0), channel_id=1, source_target_pairs={{0,24},{8,0},{16,8},{24,16},{32,56},{40,32},{48,40},{56,48},{64,88... | collective-permute-start | bytes 589832 | tf_op jit(solution)/shard_map/ppermute | solution.py:210
  67.3 0.8 collective-permute-start.1
  68.2 0.9 collective-permute-start
  69.0 6.6 %all-to-all-done.2.piece = bf16[32,8,448]{2,1,0:T(8,128)(2,1)S(1)} async-done(((bf16[32,8,448]{2,1,0:T(8,128)(2,1)}), bf16[32,8,448]{2,1,0:T(8,128)(2,1)S(1)}, u32[]{:S(2)}, u32[]{:S(2)}) %all-to-all-start.2) | async-done | bytes 229408 | tf_op jit(solution)/shard_map/all_to_all | solution.py:19
  75.7 0.9 shard_map.199
  76.5 4.8 %all-to-all-start.3 = ((f32[8,8,128]{2,1,0:T(8,128)}), f32[8,8,128]{2,1,0:T(8,128)S(1)}, u32[]{:S(2)}, u32[]{:S(2)}) async-start(f32[8,8,128]{2,1,0:T(8,128)} %shard_map.199), calls=%async_computation.3 | async-start | bytes 65536 | tf_op jit(solution)/shard_map/all_to_all | solution.py:19
  81.4 0.0 collective-permute-done.1.w2
  81.4 0.6 copy-done.8
  82.0 0.1 copy-done.9
  82.1 0.7 copy-done.10
  82.8 2.4 %shard_map.196 = (bf16[192,512]{1,0:T(8,128)(2,1)}, bf16[1024,256]{1,0:T(8,128)(2,1)}) custom-call(bf16[32,24,128]{2,1,0:T(8,128)(2,1)} %copy-done.7, bf16[32,24,128]{2,1,0:T(8,128)(2,1)} %copy-done.10, bf16[32,24,128]{2,1,0:T(8,128)(2,1)} %copy-done.9, bf16[32,24,128]{2,1,0:T(8,128)(2,1)} %copy-done.8), custom_call_target="tpu_custom_call" | custom-call | tf_op jit(solution)/shard_map/pallas_call | solution.py:33
  85.2 1.9 %shard_map.200 = (f32[16,192]{1,0:T(8,128)S(1)}, f32[32,256]{1,0:T(8,128)S(1)}, bf16[192,512]{1,0:T(8,128)(2,1)S(1)}, bf16[1024,256]{1,0:T(8,128)(2,1)S(1)}) custom-call(bf16[32,72,128]{2,1,0:T(8,128)(2,1)} %copy-done.5, bf16[32,72,128]{2,1,0:T(8,128)(2,1)} %copy-done.6, bf16[32,8,448]{2,1,0:T(8,128)(2,1)S(1)} %all-to-all-done.2.piece, ...), custom_call_target="tpu_custom_call" | custom-call | tf_op jit(solution)/shard_map/pallas_call | solution.py:33
  87.1 2.4 %shard_map.201 = (f32[16,192]{1,0:T(8,128)}, f32[32,256]{1,0:T(8,128)}, f32[16,192]{1,0:T(8,128)}, f32[32,256]{1,0:T(8,128)}, bf16[192,512]{1,0:T(8,128)(2,1)}, /*index=5*/bf16[1024,256]{1,0:T(8,128)(2,1)}) custom-call(bf16[192,512]{1,0:T(8,128)(2,1)} %get-tuple-element.27.whole_q_t, bf16[1024,256]{1,0:T(8,128)(2,1)} %get-tuple-element.28.whole_o, ...), custom_call_target="tpu_custom_call" | custom-call | tf_op jit(solution)/shard_map/pallas_call | solution.py:33
  (15 shorter events, 0.0 us)
Async XLA Ops:
  0.6 32.4 %copy-start = (bf16[3072,256]{1,0:T(8,128)(2,1)S(1)}, bf16[3072,256]{1,0:T(8,128)(2,1)}, u32[]{:S(2)}) copy-start(bf16[3072,256]{1,0:T(8,128)(2,1)} %param.15) | copy-start | bytes 4718596
  2.5 30.5 %all-to-all-start = ((bf16[32,72,128]{2,1,0:T(8,128)(2,1)}), bf16[32,72,128]{2,1,0:T(8,128)(2,1)S(1)}, u32[]{:S(2)}, u32[]{:S(2)}) async-start(bf16[32,72,128]{2,1,0:T(8,128)(2,1)} %shard_map.195), calls=%async_computation | async-start | bytes 1179648 | tf_op jit(solution)/shard_map/all_to_all | solution.py:19
  17.0 41.5 %copy-start.1 = (f32[8,192]{1,0:T(8,128)S(1)}, f32[8,192]{1,0:T(8,128)}, u32[]{:S(2)}) copy-start(f32[8,192]{1,0:T(8,128)} %mq.1) | copy-start | bytes 18436
  17.1 41.5 %copy-start.2 = (f32[8,192]{1,0:T(8,128)S(1)}, f32[8,192]{1,0:T(8,128)}, u32[]{:S(2)}) copy-start(f32[8,192]{1,0:T(8,128)} %sq.1) | copy-start | bytes 18436
  17.1 41.5 %copy-start.3 = (f32[8,256]{1,0:T(8,128)S(1)}, f32[8,256]{1,0:T(8,128)}, u32[]{:S(2)}) copy-start(f32[8,256]{1,0:T(8,128)} %mo.1) | copy-start | bytes 24580
  17.1 41.5 %copy-start.4 = (f32[8,256]{1,0:T(8,128)S(1)}, f32[8,256]{1,0:T(8,128)}, u32[]{:S(2)}) copy-start(f32[8,256]{1,0:T(8,128)} %so.1) | copy-start | bytes 24580
  33.0 4.9 %copy-start.5 = (bf16[32,72,128]{2,1,0:T(8,128)(2,1)}, bf16[32,72,128]{2,1,0:T(8,128)(2,1)S(1)}, u32[]{:S(2)}) copy-start(bf16[32,72,128]{2,1,0:T(8,128)(2,1)S(1)} %all-to-all-done.own) | copy-start | bytes 1769476
  33.0 4.9 %collective-permute-start.3 = (bf16[32,72,128]{2,1,0:T(8,128)(2,1)S(1)}, bf16[32,72,128]{2,1,0:T(8,128)(2,1)S(1)}, u32[]{:S(2)}, u32[]{:S(2)}) collective-permute-start(bf16[32,72,128]{2,1,0:T(8,128)(2,1)S(1)} %all-to-all-done.own), channel_id=1, source_target_pairs={{0,1},{1,0},{2,3},{3,2},{4,5},{5,4},{6,7},{7,6},{8,9},{9,8},{10,11... | collective-permute-start | bytes 1769480 | tf_op jit(solution)/shard_map/ppermute | solution.py:206
  37.9 0.8 copy-start.6
  59.5 16.2 %all-to-all-start.2 = ((bf16[32,8,448]{2,1,0:T(8,128)(2,1)}), bf16[32,8,448]{2,1,0:T(8,128)(2,1)S(1)}, u32[]{:S(2)}, u32[]{:S(2)}) async-start(bf16[32,8,448]{2,1,0:T(8,128)(2,1)} %get-tuple-element.29), calls=%async_computation.2 | async-start | bytes 524288 | tf_op jit(solution)/shard_map/all_to_all | solution.py:19
  64.3 17.1 %copy-start.7 = (bf16[32,24,128]{2,1,0:T(8,128)(2,1)}, bf16[32,24,128]{2,1,0:T(8,128)(2,1)S(1)}, u32[]{:S(2)}) copy-start(bf16[32,24,128]{2,1,0:T(8,128)(2,1)S(1)} %slice.4.w0) | copy-start | bytes 589828
  64.3 17.0 %collective-permute-start.2 = (bf16[32,24,128]{2,1,0:T(8,128)(2,1)S(1)}, bf16[32,24,128]{2,1,0:T(8,128)(2,1)S(1)}, u32[]{:S(2)}, u32[]{:S(2)}) collective-permute-start(bf16[32,24,128]{2,1,0:T(8,128)(2,1)S(1)} %slice.4.w0), channel_id=1, source_target_pairs={{0,24},{8,0},{16,8},{24,16},{32,56},{40,32},{48,40},{56,48},{64,88... | collective-permute-start | bytes 589832 | tf_op jit(solution)/shard_map/ppermute | solution.py:210
  67.3 14.0 %collective-permute-start.1 = (bf16[32,24,128]{2,1,0:T(8,128)(2,1)S(1)}, bf16[32,24,128]{2,1,0:T(8,128)(2,1)S(1)}, u32[]{:S(2)}, u32[]{:S(2)}) collective-permute-start(bf16[32,24,128]{2,1,0:T(8,128)(2,1)S(1)} %slice.4.w0), channel_id=1, source_target_pairs={{0,16},{8,24},{16,0},{24,8},{32,48},{40,56},{48,32},{56,40},{64,80... | collective-permute-start | bytes 589832 | tf_op jit(solution)/shard_map/ppermute | solution.py:210
  68.2 13.2 %collective-permute-start = (bf16[32,24,128]{2,1,0:T(8,128)(2,1)S(1)}, bf16[32,24,128]{2,1,0:T(8,128)(2,1)S(1)}, u32[]{:S(2)}, u32[]{:S(2)}) collective-permute-start(bf16[32,24,128]{2,1,0:T(8,128)(2,1)S(1)} %slice.4.w0), channel_id=1, source_target_pairs={{0,8},{8,16},{16,24},{24,0},{32,40},{40,48},{48,56},{56,32},{64,72... | collective-permute-start | bytes 589832 | tf_op jit(solution)/shard_map/ppermute | solution.py:210
  76.5 10.6 %all-to-all-start.3 = ((f32[8,8,128]{2,1,0:T(8,128)}), f32[8,8,128]{2,1,0:T(8,128)S(1)}, u32[]{:S(2)}, u32[]{:S(2)}) async-start(f32[8,8,128]{2,1,0:T(8,128)} %shard_map.199), calls=%async_computation.3 | async-start | bytes 65536 | tf_op jit(solution)/shard_map/all_to_all | solution.py:19
  81.3 0.7 copy-start.8
  81.4 0.7 copy-start.9
  82.1 0.7 copy-start.10

commit v4 on v3

--- a/solution.py
+++ b/solution.py
@@ -12,11 +12,15 @@
 F32 = jnp.float32
 LANES = 128
 SMALL = 16 * 2**20
+FIRST = (6, 2)
 RING = 4
 
 
-def exchange(tiles, axis):
-    return lax.all_to_all(tiles, axis, split_axis=0, concat_axis=0, tiled=True)
+def exchange(tiles, axis, order=None):
+    groups = None if order is None else [order]
+    return lax.all_to_all(
+        tiles, axis, split_axis=0, concat_axis=0, tiled=True, axis_index_groups=groups
+    )
 
 
 def contract(left, right, left_dim, right_dim):
@@ -28,13 +32,17 @@
     return pltpu.with_memory_space_constraint(x, pltpu.VMEM)
 
 
-def on_chip(body, outs, *args, scratch=(), limit=None, copied=False):
+FAR, NEAR, BY_HAND = "far", "near", "by hand"
+
+
+def on_chip(body, outs, *args, scratch=(), limit=None):
     vmem = pl.BlockSpec(memory_space=pltpu.VMEM)
+    hand = pl.BlockSpec(memory_space=pl.ANY)
     return pl.pallas_call(
         body,
-        out_shape=tuple(pltpu.VMEM(s, d) if stays else jax.ShapeDtypeStruct(s, d) for s, d, stays in outs),
+        out_shape=tuple(pltpu.VMEM(s, d) if at == NEAR else jax.ShapeDtypeStruct(s, d) for s, d, at in outs),
         in_specs=[vmem] * len(args),
-        out_specs=tuple(pl.BlockSpec(memory_space=pl.ANY) if copied else vmem for _ in outs),
+        out_specs=tuple(hand if at == BY_HAND else vmem for _, _, at in outs),
         scratch_shapes=list(scratch),
         compiler_params=pltpu.CompilerParams(vmem_limit_bytes=limit),
     )(*args)
@@ -42,6 +50,28 @@
 
 def halves(x):
     return x[:, :LANES], x[:, LANES:]
+
+
+def turned(x, by, axis):
+    size = x.shape[axis]
+    by %= size
+    if by == 0:
+        return x
+    return jnp.concatenate(
+        [lax.slice_in_dim(x, size - by, size, axis=axis), lax.slice_in_dim(x, 0, size - by, axis=axis)], axis=axis
+    )
+
+
+def in_order(x, back=False):
+    x = x.reshape(-1, RING, *x.shape[1:])
+    for axis, by in enumerate(FIRST):
+        x = turned(x, -by if back else by, axis)
+    return x.reshape(-1, *x.shape[2:])
+
+
+def exchange_order(count):
+    z, y = FIRST
+    return [(i // RING + z) % (count // RING) * RING + (i + y) % RING for i in range(count)]
 
 
 def pack_body(fq, fo, wq, wo, out, tiles, sems):
@@ -55,11 +85,12 @@
             left, right = halves(f[...])
             half = jnp.where(core == 0, left.astype(F32), right.astype(F32)).astype(BF16)
             tiles[y, at : at + f.shape[0]] = half
-        row, col = y % 2, y // 2
+        to = (y + FIRST[1]) % RING
+        row, col = to % 2, to // 2
         part = wq[8 * row : 8 * row + 8, col * LANES : min(width_q, (col + 1) * LANES)]
         if part.shape[1] < LANES:
             part = jnp.concatenate([part, jnp.zeros((8, LANES - part.shape[1]), F32)], axis=1)
-        left, right = halves(wo[8 * y : 8 * y + 8, :])
+        left, right = halves(wo[8 * to : 8 * to + 8, :])
         tiles[y, rows:] = jnp.concatenate([part, left, right], axis=0).astype(BF16)
     copies = [
         pltpu.make_async_copy(tiles, out.at[pl.ds(z * RING, RING)], sems.at[z])
@@ -75,15 +106,30 @@
     count = own.shape[0]
     core = lax.axis_index("tp") % 2
     width_q = gq_t.shape[0]
-    part = (count // 2, LANES * 2 // count, -1)
-    for ref, at in ((own, core), (other, 1 - core)):
-        fq = ref[:, :rows_q].reshape(count * rows_q, LANES)
-        fo = ref[:, rows_q:rows].reshape(count * (rows - rows_q), LANES)
+    lows = []
+    for ref in (own, other):
+        fq = in_order(ref[:, :rows_q]).reshape(count * rows_q, LANES)
+        fo = in_order(ref[:, rows_q:rows]).reshape(count * (rows - rows_q), LANES)
         low_q = contract(gq_t[...], fq, 1, 0).T * inv_root
         low_o = contract(fo, go[...], 0, 0) * inv_root
-        to = pl.ds(at * (count // 2), count // 2)
-        out[to, :, :width_q] = low_q.reshape(part).astype(BF16)
-        out[to, :, width_q:] = low_o.reshape(part).astype(BF16)
+        lows.append((low_q, low_o))
+    for mine, others, at in zip(*lows, (slice(0, width_q), slice(width_q, None))):
+        low = jnp.concatenate(
+            [jnp.where(core == 0, mine, others), jnp.where(core == 0, others, mine)], axis=0
+        )
+        out[:, :, at] = in_order(low.reshape(count, -1, low.shape[1]), back=True).astype(BF16)
+
+
+def keep_body(own, other, kept, sems):
+    core = lax.axis_index("tp") % 2
+    copies = [
+        pltpu.make_async_copy(ref, kept.at[at], sems.at[k])
+        for k, (ref, at) in enumerate(((own, core), (other, 1 - core)))
+    ]
+    for copy in copies:
+        copy.start()
+    for copy in copies:
+        copy.wait()
 
 
 def moments_body(parts, mq, sq, mo, so, mq_new, sq_new, mo_new, so_new, out):
@@ -110,24 +156,23 @@
     out[:, half[1] :] = jnp.broadcast_to(jnp.sum(squares[:, width_q:], keepdims=True)[None], half)
 
 
-def product_body(own, other, piece, fq_own, fo_own, step_q, step_o, all_q, all_o):
-    core = lax.axis_index("tp") % 2
+def product_body(kept, piece, fq_own, fo_own, step_q, step_o, all_q_t, all_o):
     rows_q, width_q = step_q.shape
     rows = rows_q + step_o.shape[0]
-    count = own.shape[0]
+    count = kept.shape[1]
     rank = fq_own.shape[1]
-    whole = piece[...].reshape(rank, -1)
+    whole = in_order(piece[...]).reshape(rank, -1)
     step_q[...] = contract(fq_own[...], whole[:, :width_q], 1, 0)
     step_o[...] = contract(fo_own[...], whole[:, width_q:], 1, 0)
     step_all_q = 0.0
     step_all_o = 0.0
-    for ref, at in ((own, core), (other, 1 - core)):
-        direction = piece[pl.ds(at * (count // 2), count // 2)].reshape(LANES, -1)
-        fq = ref[:, :rows_q].reshape(count * rows_q, LANES)
-        fo = ref[:, rows_q:rows].reshape(count * (rows - rows_q), LANES)
+    for core in range(2):
+        direction = whole[core * LANES : (core + 1) * LANES]
+        fq = in_order(kept[core, :, :rows_q]).reshape(count * rows_q, LANES)
+        fo = in_order(kept[core, :, rows_q:rows]).reshape(count * (rows - rows_q), LANES)
         step_all_q = step_all_q + contract(fq, direction[:, :width_q], 1, 0)
         step_all_o = step_all_o + contract(fo, direction[:, width_q:], 1, 0)
-    all_q[...] = step_all_q.T.astype(BF16)
+    all_q_t[...] = step_all_q.T.astype(BF16)
     all_o[...] = step_all_o.astype(BF16)
 
 
@@ -136,7 +181,7 @@
     width_q = whole_q_t.shape[0]
     for k, ref in enumerate((w0, w1, w2, w3)):
         u = (y + (RING - k)) % RING
-        got = ref[...].astype(F32)
+        got = in_order(ref[...].astype(F32))
         held_q[u // 2, :, u % 2] = got[:, 0:8]
         held_o[0, :, u] = got[:, 8:16]
         held_o[1, :, u] = got[:, 16:24]
@@ -192,15 +237,14 @@
 
     (packed,) = on_chip(
         pack_body,
-        [((count, rows + quarter, LANES), BF16, False)],
+        [((count, rows + quarter, LANES), BF16, BY_HAND)],
         query_factor, output_factor, query_weight, output_weight,
         scratch=(
             pltpu.VMEM((RING, rows + quarter, LANES), BF16),
             pltpu.SemaphoreType.DMA((count // RING,)),
         ),
-        copied=True,
-    )
-    own = exchange(packed, "fs")
+    )
+    own = exchange(packed, "fs", exchange_order(count))
     grad_q_t = contract(query_cot, latent_in, 0, 0).astype(BF16)
     grad_o = contract(attn_out, mix_cot, 0, 0).astype(BF16)
     other = lax.ppermute(own, "tp", [(i, i ^ 1) for i in range(columns)])
@@ -211,21 +255,27 @@
 
     (low,) = on_chip(
         functools.partial(low_body, inv_root, rows_q, rows),
-        [((count, rank // count, width), BF16, True)],
-        own, other, near(grad_q_t), near(grad_o),
-    )
-    parts = exchange(low, "fs")
-    of_q = (query_mean.shape, F32, False)
-    of_o = (output_mean.shape, F32, False)
+        [((count, rank // count, width), BF16, FAR)],
+        near(own), near(other), near(grad_q_t), near(grad_o),
+    )
+    (kept,) = on_chip(
+        keep_body,
+        [((2, *own.shape), BF16, BY_HAND)],
+        near(own), near(other),
+        scratch=(pltpu.SemaphoreType.DMA((2,)),),
+    )
+    parts = exchange(low, "fs", exchange_order(count))
+    of_q = (query_mean.shape, F32, FAR)
+    of_o = (output_mean.shape, F32, FAR)
     mean_q, square_q, mean_o, square_o, joined = on_chip(
         moments_body,
-        [of_q, of_q, of_o, of_o, ((count, rank // count, width), BF16, False)],
+        [of_q, of_q, of_o, of_o, ((count, rank // count, width), BF16, FAR)],
         near(parts), query_mean, query_square, output_mean, output_square, limit=SMALL,
     )
-    piece = exchange(joined, "fs")
+    piece = exchange(joined, "fs", exchange_order(count))
     wholes = on_chip(
         assemble_body,
-        [((width_q, rows_q * count), BF16, False), ((rows_o * count, width_o), BF16, False)],
+        [((width_q, rows_q * count), BF16, FAR), ((rows_o * count, width_o), BF16, FAR)],
         *held,
         scratch=(
             pltpu.VMEM((2, count, 2, 8, LANES), F32),
@@ -233,29 +283,29 @@
         ),
     )
     (sums,) = on_chip(
-        functools.partial(sums_body, width_q), [((columns, 8, LANES), F32, False)], near(piece), limit=SMALL
-    )
-    sums = exchange(sums, "tp")
+        functools.partial(sums_body, width_q), [((columns, 8, LANES), F32, FAR)], near(piece), limit=SMALL
+    )
+    sums = exchange(sums, "tp", [i ^ 5 for i in range(columns)])
     sizes = (rank * width_q * columns, rank * width_o * columns)
     products = on_chip(
         product_body,
         [
-            ((rows_q, width_q), F32, True),
-            ((rows_o, width_o), F32, True),
-            ((width_q, rows_q * count), BF16, True),
-            ((rows_o * count, width_o), BF16, True),
+            ((rows_q, width_q), F32, NEAR),
+            ((rows_o, width_o), F32, NEAR),
+            ((width_q, rows_q * count), BF16, NEAR),
+            ((rows_o * count, width_o), BF16, NEAR),
         ],
-        own, other, near(piece), query_factor, output_factor,
+        kept, near(piece), query_factor, output_factor,
     )
     step_q, step_o, new_q, new_o, copy_q_t, copy_o = on_chip(
         functools.partial(final_body, sizes),
         [
-            ((rows_q, width_q), F32, False),
-            ((rows_o, width_o), F32, False),
-            ((rows_q, width_q), F32, False),
-            ((rows_o, width_o), F32, False),
-            ((width_q, rows_q * count), BF16, False),
-            ((rows_o * count, width_o), BF16, False),
+            ((rows_q, width_q), F32, FAR),
+            ((rows_o, width_o), F32, FAR),
+            ((rows_q, width_q), F32, FAR),
+            ((rows_o, width_o), F32, FAR),
+            ((width_q, rows_q * count), BF16, FAR),
+            ((rows_o * count, width_o), BF16, FAR),
         ],
         *wholes, near(sums), *map(near, products), query_weight, output_weight,
     )

time: 91 us -> 88.8 us (0.976)
  the two profiles are of different devices: /device:TPU:2 before, /device:TPU:1 now
where the time goes in v4:
time: 88.8 us; the launch traced here: 88.2 us
  starting transfers between devices  33.5 us (38%)
  blocking collectives  16.5 us (19%)
  waiting for transfers between devices  14.5 us (16%)
  Pallas kernels  12.6 us (14%)
  matrix products  7.65 us (9%)
  local copies, waits for them, and re-layouts  2.54 us (3%)
    all_to_all x3, starting transfers between devices, exchange(): lax.all_to_all(tiles, axis, split_axis=0, concat_axis=0, tiled=True, axis...  29.4 us
    all_to_all x1, blocking collectives, exchange(): lax.all_to_all(tiles, axis, split_axis=0, concat_axis=0, tiled=True, axis...  16.5 us
    all_to_all x3, waiting for transfers between devices, exchange(): lax.all_to_all(tiles, axis, split_axis=0, concat_axis=0, tiled=True, axis...  14.5 us
    pallas_call x8, Pallas kernels, on_chip(): pl.pallas_call(body, out_shape=tuple((pltpu.VMEM(s, d) if at == NEAR else...  12.6 us
    dot_general x2, matrix products, contract(): return lax.dot_general(left, right, dims, preferred_element_type=F32)  7.65 us
    ppermute x1, starting transfers between devices, on_device(): other = lax.ppermute(own, 'tp', [(i, i ^ 1) for i in range(columns)])  2.55 us
    unnamed x18, local copies, waits for them, and re-layouts  2.51 us
  transfers between devices with their start and end apart: 7, of which 2 were waited for; matrix products, arithmetic and copies ran while one was open for 9% of the time, Pallas kernels for 7%

profile of v4, /device:TPU:1, one launch (start us, length us, event | category | flops | bytes accessed | tf_op | source)
XLA Modules:
  0.0 88.2 jit_solution(7352184167043278326)
XLA Ops:
  0.6 0.0 copy-start
  0.7 1.8 %shard_map.195 = bf16[32,72,128]{2,1,0:T(8,128)(2,1)} custom-call(bf16[16,256]{1,0:T(8,128)(2,1)} %fq_own.1, bf16[32,256]{1,0:T(8,128)(2,1)} %fo_own.1, f32[16,192]{1,0:T(8,128)} %wq.3, f32[32,256]{1,0:T(8,128)} %wo.3), custom_call_target="tpu_custom_call" | custom-call | tf_op jit(solution)/shard_map/pallas_call | solution.py:41
  2.5 13.1 %all-to-all-start = ((bf16[32,72,128]{2,1,0:T(8,128)(2,1)}), bf16[32,72,128]{2,1,0:T(8,128)(2,1)S(1)}, u32[]{:S(2)}, u32[]{:S(2)}) async-start(bf16[32,72,128]{2,1,0:T(8,128)(2,1)} %shard_map.195), calls=%async_computation | async-start | bytes 1179648 | tf_op jit(solution)/shard_map/all_to_all | solution.py:21
  15.6 3.0 %convolution_convert_fusion.1.gq_t = bf16[192,512]{1,0:T(8,128)(2,1)S(1)} fusion(bf16[3072,192]{0,1:T(8,128)(2,1)} %param.13, bf16[3072,512]{1,0:T(8,128)(2,1)} %param.12), kind=kOutput, calls=%fused_computation.1 | convolution fusion | flops 604078080 | bytes 4521984 | tf_op jit(solution)/shard_map/dot_general | solution.py:28
  18.6 9.9 %all-to-all-done.own = bf16[32,72,128]{2,1,0:T(8,128)(2,1)S(1)} async-done(((bf16[32,72,128]{2,1,0:T(8,128)(2,1)}), bf16[32,72,128]{2,1,0:T(8,128)(2,1)S(1)}, u32[]{:S(2)}, u32[]{:S(2)}) %all-to-all-start) | async-done | bytes 589856 | tf_op jit(solution)/shard_map/all_to_all | solution.py:21
  28.5 2.5 %collective-permute-start.3 = (bf16[32,72,128]{2,1,0:T(8,128)(2,1)S(1)}, bf16[32,72,128]{2,1,0:T(8,128)(2,1)S(1)}, u32[]{:S(2)}, u32[]{:S(2)}) collective-permute-start(bf16[32,72,128]{2,1,0:T(8,128)(2,1)S(1)} %all-to-all-done.own), channel_id=1, source_target_pairs={{0,1},{1,0},{2,3},{3,2},{4,5},{5,4},{6,7},{7,6},{8,9},{9,8},{10,11... | collective-permute-start | bytes 1769480 | tf_op jit(solution)/shard_map/ppermute | solution.py:250
  31.1 4.6 %convolution_convert_fusion.go = bf16[1024,256]{1,0:T(8,128)(2,1)S(1)} fusion(bf16[3072,1024]{1,0:T(8,128)(2,1)} %param.14, bf16[3072,256]{1,0:T(8,128)(2,1)S(1)} %copy-done), kind=kOutput, calls=%fused_computation | convolution fusion | flops 1610874880 | bytes 8388608 | tf_op jit(solution)/shard_map/dot_general | solution.py:28
  35.7 0.0 copy-start.3
  35.7 0.0 copy-start.4
  35.8 0.0 copy-start.5
  35.8 0.0 copy-start.6
  35.8 1.2 %shard_map.197 = bf16[32,8,448]{2,1,0:T(8,128)(2,1)} custom-call(bf16[32,72,128]{2,1,0:T(8,128)(2,1)S(1)} %all-to-all-done.own, bf16[32,72,128]{2,1,0:T(8,128)(2,1)S(1)} %collective-permute-done.3.other, bf16[192,512]{1,0:T(8,128)(2,1)S(1)} %convolution_convert_fusion.1.gq_t, bf16[1024,256]{1,0:T(8,128)(2,1)S(1)} %convolution_convert_fusion.go), custom_call_target="tpu_custom_call" | custom-call | tf_op jit(solution)/shard_map/pallas_call | solution.py:41
  37.0 16.5 %all_to_all.20.parts = bf16[32,8,448]{2,1,0:T(8,128)(2,1)S(1)} all-to-all(bf16[32,8,448]{2,1,0:T(8,128)(2,1)} %shard_map.197), channel_id=1, replica_groups={{208,216,192,200,240,248,224,232,16,24,0,8,48,56,32,40,80,88,64,72,112,..., dimensions={0} | all-to-all | bytes 458752 | tf_op jit(solution)/shard_map/all_to_all | solution.py:21
  53.5 0.9 %shard_map.198 = (f32[8,192]{1,0:T(8,128)}, f32[8,192]{1,0:T(8,128)}, f32[8,256]{1,0:T(8,128)}, f32[8,256]{1,0:T(8,128)}, bf16[32,8,448]{2,1,0:T(8,128)(2,1)}) custom-call(bf16[32,8,448]{2,1,0:T(8,128)(2,1)S(1)} %all_to_all.20.parts, f32[8,192]{1,0:T(8,128)S(1)} %copy-done.3, f32[8,192]{1,0:T(8,128)S(1)} %copy-done.4, f32[8,256]{1,0:T(8,128)S(1)} %copy-done.5, ...), custom_call_target="tpu_custom_call" | custom-call | tf_op jit(solution)/shard_map/pallas_call | solution.py:41
  54.5 8.5 %all-to-all-start.2 = ((bf16[32,8,448]{2,1,0:T(8,128)(2,1)}), bf16[32,8,448]{2,1,0:T(8,128)(2,1)S(1)}, u32[]{:S(2)}, u32[]{:S(2)}) async-start(bf16[32,8,448]{2,1,0:T(8,128)(2,1)} %get-tuple-element.29), calls=%async_computation.2 | async-start | bytes 524288 | tf_op jit(solution)/shard_map/all_to_all | solution.py:21
  63.0 0.0 copy-start.7
  63.0 0.4 collective-permute-start.2
  63.4 1.2 %collective-permute-start.1 = (bf16[32,24,128]{2,1,0:T(8,128)(2,1)S(1)}, bf16[32,24,128]{2,1,0:T(8,128)(2,1)}, u32[]{:S(2)}, u32[]{:S(2)}) collective-permute-start(bf16[32,24,128]{2,1,0:T(8,128)(2,1)S(1)} %slice.4.w0), channel_id=1, source_target_pairs={{0,16},{8,24},{16,0},{24,8},{32,48},{40,56},{48,32},{56,40},{64,80... | collective-permute-start | bytes 589832 | tf_op jit(solution)/shard_map/ppermute | solution.py:254
  64.6 0.0 collective-permute-start
  64.6 4.6 %all-to-all-done.2.piece = bf16[32,8,448]{2,1,0:T(8,128)(2,1)S(1)} async-done(((bf16[32,8,448]{2,1,0:T(8,128)(2,1)}), bf16[32,8,448]{2,1,0:T(8,128)(2,1)S(1)}, u32[]{:S(2)}, u32[]{:S(2)}) %all-to-all-start.2) | async-done | bytes 229408 | tf_op jit(solution)/shard_map/all_to_all | solution.py:21
  69.2 0.9 shard_map.199
  70.0 7.8 %all-to-all-start.3 = ((f32[8,8,128]{2,1,0:T(8,128)}), f32[8,8,128]{2,1,0:T(8,128)S(1)}, u32[]{:S(2)}, u32[]{:S(2)}) async-start(f32[8,8,128]{2,1,0:T(8,128)} %shard_map.199), calls=%async_computation.3 | async-start | bytes 65536 | tf_op jit(solution)/shard_map/all_to_all | solution.py:21
  77.9 0.0 collective-permute-done.1.w2
  77.9 0.6 copy-done.8
  78.6 2.4 %shard_map.196 = (bf16[192,512]{1,0:T(8,128)(2,1)}, bf16[1024,256]{1,0:T(8,128)(2,1)}) custom-call(bf16[32,24,128]{2,1,0:T(8,128)(2,1)} %copy-done.7, bf16[32,24,128]{2,1,0:T(8,128)(2,1)} %collective-permute-done.w1, bf16[32,24,128]{2,1,0:T(8,128)(2,1)} %collective-permute-done.1.w2, bf16[32,24,128]{2,1,0:T(8,128)(2,1)} %copy-done.8), custom_call_target="tpu_custom_call" | custom-call | tf_op jit(solution)/shard_map/pallas_call | solution.py:41
  81.0 1.0 %shard_map.200.kept = bf16[2,32,72,128]{3,2,1,0:T(8,128)(2,1)} custom-call(bf16[32,72,128]{2,1,0:T(8,128)(2,1)S(1)} %all-to-all-done.own, bf16[32,72,128]{2,1,0:T(8,128)(2,1)S(1)} %collective-permute-done.3.other), custom_call_target="tpu_custom_call" | custom-call | tf_op jit(solution)/shard_map/pallas_call | solution.py:41
  82.0 1.9 %shard_map.201 = (f32[16,192]{1,0:T(8,128)S(1)}, f32[32,256]{1,0:T(8,128)S(1)}, bf16[192,512]{1,0:T(8,128)(2,1)S(1)}, bf16[1024,256]{1,0:T(8,128)(2,1)S(1)}) custom-call(bf16[2,32,72,128]{3,2,1,0:T(8,128)(2,1)} %shard_map.200.kept, bf16[32,8,448]{2,1,0:T(8,128)(2,1)S(1)} %all-to-all-done.2.piece, bf16[16,256]{1,0:T(8,128)(2,1)} %fq_own.1, bf16[32,256]{1,0:T(8,128)(2,1)} %fo_own.1), custom_call_target="tpu_custom_call" | custom-call | tf_op jit(solution)/shard_map/pallas_call | solution.py:41
  84.0 0.0 copy-start.1
  84.0 0.8 copy-done.1
  84.8 0.0 all-to-all-done.3.sums
  84.8 1.0 %copy-done.2 = bf16[1024,256]{1,0:T(8,128)(2,1)S(1)} copy-done((bf16[1024,256]{1,0:T(8,128)(2,1)S(1)}, bf16[1024,256]{1,0:T(8,128)(2,1)}, u32[]{:S(2)}) %copy-start.2) | copy-done | bytes 524312
  85.8 2.4 %shard_map.202 = (f32[16,192]{1,0:T(8,128)}, f32[32,256]{1,0:T(8,128)}, f32[16,192]{1,0:T(8,128)}, f32[32,256]{1,0:T(8,128)}, bf16[192,512]{1,0:T(8,128)(2,1)}, /*index=5*/bf16[1024,256]{1,0:T(8,128)(2,1)}) custom-call(bf16[192,512]{1,0:T(8,128)(2,1)} %get-tuple-element.27.whole_q_t, bf16[1024,256]{1,0:T(8,128)(2,1)} %get-tuple-element.28.whole_o, ...), custom_call_target="tpu_custom_call" | custom-call | tf_op jit(solution)/shard_map/pallas_call | solution.py:41
  (12 shorter events, 0.0 us)
Async XLA Ops:
  0.6 30.5 %copy-start = (bf16[3072,256]{1,0:T(8,128)(2,1)S(1)}, bf16[3072,256]{1,0:T(8,128)(2,1)}, u32[]{:S(2)}) copy-start(bf16[3072,256]{1,0:T(8,128)(2,1)} %param.15) | copy-start | bytes 4718596
  2.5 26.1 %all-to-all-start = ((bf16[32,72,128]{2,1,0:T(8,128)(2,1)}), bf16[32,72,128]{2,1,0:T(8,128)(2,1)S(1)}, u32[]{:S(2)}, u32[]{:S(2)}) async-start(bf16[32,72,128]{2,1,0:T(8,128)(2,1)} %shard_map.195), calls=%async_computation | async-start | bytes 1179648 | tf_op jit(solution)/shard_map/all_to_all | solution.py:21
  28.5 7.2 %collective-permute-start.3 = (bf16[32,72,128]{2,1,0:T(8,128)(2,1)S(1)}, bf16[32,72,128]{2,1,0:T(8,128)(2,1)S(1)}, u32[]{:S(2)}, u32[]{:S(2)}) collective-permute-start(bf16[32,72,128]{2,1,0:T(8,128)(2,1)S(1)} %all-to-all-done.own), channel_id=1, source_target_pairs={{0,1},{1,0},{2,3},{3,2},{4,5},{5,4},{6,7},{7,6},{8,9},{9,8},{10,11... | collective-permute-start | bytes 1769480 | tf_op jit(solution)/shard_map/ppermute | solution.py:250
  35.7 17.8 %copy-start.3 = (f32[8,192]{1,0:T(8,128)S(1)}, f32[8,192]{1,0:T(8,128)}, u32[]{:S(2)}) copy-start(f32[8,192]{1,0:T(8,128)} %mq.1) | copy-start | bytes 18436
  35.7 17.8 %copy-start.4 = (f32[8,192]{1,0:T(8,128)S(1)}, f32[8,192]{1,0:T(8,128)}, u32[]{:S(2)}) copy-start(f32[8,192]{1,0:T(8,128)} %sq.1) | copy-start | bytes 18436
  35.8 17.8 %copy-start.5 = (f32[8,256]{1,0:T(8,128)S(1)}, f32[8,256]{1,0:T(8,128)}, u32[]{:S(2)}) copy-start(f32[8,256]{1,0:T(8,128)} %mo.1) | copy-start | bytes 24580
  35.8 17.8 %copy-start.6 = (f32[8,256]{1,0:T(8,128)S(1)}, f32[8,256]{1,0:T(8,128)}, u32[]{:S(2)}) copy-start(f32[8,256]{1,0:T(8,128)} %so.1) | copy-start | bytes 24580
  54.5 14.7 %all-to-all-start.2 = ((bf16[32,8,448]{2,1,0:T(8,128)(2,1)}), bf16[32,8,448]{2,1,0:T(8,128)(2,1)S(1)}, u32[]{:S(2)}, u32[]{:S(2)}) async-start(bf16[32,8,448]{2,1,0:T(8,128)(2,1)} %get-tuple-element.29), calls=%async_computation.2 | async-start | bytes 524288 | tf_op jit(solution)/shard_map/all_to_all | solution.py:21
  63.0 14.9 %copy-start.7 = (bf16[32,24,128]{2,1,0:T(8,128)(2,1)}, bf16[32,24,128]{2,1,0:T(8,128)(2,1)S(1)}, u32[]{:S(2)}) copy-start(bf16[32,24,128]{2,1,0:T(8,128)(2,1)S(1)} %slice.4.w0) | copy-start | bytes 589828
  63.0 14.8 %collective-permute-start.2 = (bf16[32,24,128]{2,1,0:T(8,128)(2,1)S(1)}, bf16[32,24,128]{2,1,0:T(8,128)(2,1)S(1)}, u32[]{:S(2)}, u32[]{:S(2)}) collective-permute-start(bf16[32,24,128]{2,1,0:T(8,128)(2,1)S(1)} %slice.4.w0), channel_id=1, source_target_pairs={{0,24},{8,0},{16,8},{24,16},{32,56},{40,32},{48,40},{56,48},{64,88... | collective-permute-start | bytes 589832 | tf_op jit(solution)/shard_map/ppermute | solution.py:254
  63.4 14.5 %collective-permute-start.1 = (bf16[32,24,128]{2,1,0:T(8,128)(2,1)S(1)}, bf16[32,24,128]{2,1,0:T(8,128)(2,1)}, u32[]{:S(2)}, u32[]{:S(2)}) collective-permute-start(bf16[32,24,128]{2,1,0:T(8,128)(2,1)S(1)} %slice.4.w0), channel_id=1, source_target_pairs={{0,16},{8,24},{16,0},{24,8},{32,48},{40,56},{48,32},{56,40},{64,80... | collective-permute-start | bytes 589832 | tf_op jit(solution)/shard_map/ppermute | solution.py:254
  64.6 13.3 %collective-permute-start = (bf16[32,24,128]{2,1,0:T(8,128)(2,1)S(1)}, bf16[32,24,128]{2,1,0:T(8,128)(2,1)}, u32[]{:S(2)}, u32[]{:S(2)}) collective-permute-start(bf16[32,24,128]{2,1,0:T(8,128)(2,1)S(1)} %slice.4.w0), channel_id=1, source_target_pairs={{0,8},{8,16},{16,24},{24,0},{32,40},{40,48},{48,56},{56,32},{64,72... | collective-permute-start | bytes 589832 | tf_op jit(solution)/shard_map/ppermute | solution.py:254
  70.0 14.7 %all-to-all-start.3 = ((f32[8,8,128]{2,1,0:T(8,128)}), f32[8,8,128]{2,1,0:T(8,128)S(1)}, u32[]{:S(2)}, u32[]{:S(2)}) async-start(f32[8,8,128]{2,1,0:T(8,128)} %shard_map.199), calls=%async_computation.3 | async-start | bytes 65536 | tf_op jit(solution)/shard_map/all_to_all | solution.py:21
  77.9 0.7 copy-start.8
  84.0 0.8 copy-start.1
  84.8 1.0 %copy-start.2 = (bf16[1024,256]{1,0:T(8,128)(2,1)S(1)}, bf16[1024,256]{1,0:T(8,128)(2,1)}, u32[]{:S(2)}) copy-start(bf16[1024,256]{1,0:T(8,128)(2,1)} %copy-done.1) | copy-start | bytes 1572868

commit v5 on v4

--- a/solution.py
+++ b/solution.py
@@ -12,7 +12,7 @@
 F32 = jnp.float32
 LANES = 128
 SMALL = 16 * 2**20
-FIRST = (6, 2)
+FIRST, LOW, DIRECTION = (5, 2), (5, 2), (4, 2)
 RING = 4
 
 
@@ -62,16 +62,27 @@
     )
 
 
-def in_order(x, back=False):
+def in_order(x, first, back=False):
     x = x.reshape(-1, RING, *x.shape[1:])
-    for axis, by in enumerate(FIRST):
+    for axis, by in enumerate(first):
         x = turned(x, -by if back else by, axis)
     return x.reshape(-1, *x.shape[2:])
 
 
-def exchange_order(count):
-    z, y = FIRST
+def exchange_order(count, first):
+    z, y = first
     return [(i // RING + z) % (count // RING) * RING + (i + y) % RING for i in range(count)]
+
+
+def folded(q, o):
+    return jnp.concatenate([o[..., :4, :], o[..., 4:, :], q[..., :4, :], q[..., 4:, :]], axis=-1)
+
+
+def unfolded(x, width_q):
+    at = x.shape[-1] - 2 * width_q
+    o = jnp.concatenate([x[..., : at // 2], x[..., at // 2 : at]], axis=-2)
+    q = jnp.concatenate([x[..., at : at + width_q], x[..., at + width_q :]], axis=-2)
+    return q, o
 
 
 def pack_body(fq, fo, wq, wo, out, tiles, sems):
@@ -105,19 +116,20 @@
 def low_body(inv_root, rows_q, rows, own, other, gq_t, go, out):
     count = own.shape[0]
     core = lax.axis_index("tp") % 2
-    width_q = gq_t.shape[0]
     lows = []
     for ref in (own, other):
-        fq = in_order(ref[:, :rows_q]).reshape(count * rows_q, LANES)
-        fo = in_order(ref[:, rows_q:rows]).reshape(count * (rows - rows_q), LANES)
+        fq = in_order(ref[:, :rows_q], FIRST).reshape(count * rows_q, LANES)
+        fo = in_order(ref[:, rows_q:rows], FIRST).reshape(count * (rows - rows_q), LANES)
         low_q = contract(gq_t[...], fq, 1, 0).T * inv_root
         low_o = contract(fo, go[...], 0, 0) * inv_root
         lows.append((low_q, low_o))
-    for mine, others, at in zip(*lows, (slice(0, width_q), slice(width_q, None))):
+    whole = []
+    for mine, others in zip(*lows):
         low = jnp.concatenate(
             [jnp.where(core == 0, mine, others), jnp.where(core == 0, others, mine)], axis=0
         )
-        out[:, :, at] = in_order(low.reshape(count, -1, low.shape[1]), back=True).astype(BF16)
+        whole.append(in_order(low.reshape(count, -1, low.shape[1]), LOW, back=True))
+    out[...] = folded(*whole).astype(BF16)
 
 
 def keep_body(own, other, kept, sems):
@@ -133,27 +145,27 @@
 
 
 def moments_body(parts, mq, sq, mo, so, mq_new, sq_new, mo_new, so_new, out):
-    low = jnp.sum(parts[...].astype(F32), axis=0)
-    width_q = mq.shape[1]
-    count = out.shape[0]
-    for piece, mean, square, mean_out, square_out, at in (
-        (low[:, :width_q], mq, sq, mq_new, sq_new, slice(0, width_q)),
-        (low[:, width_q:], mo, so, mo_new, so_new, slice(width_q, None)),
+    low_q, low_o = unfolded(jnp.sum(parts[...].astype(F32), axis=0), mq.shape[1])
+    directions = []
+    for low, mean, square, mean_out, square_out in (
+        (low_q, mq, sq, mq_new, sq_new),
+        (low_o, mo, so, mo_new, so_new),
     ):
-        mean_new = 0.8 * mean[...] + 0.2 * piece
-        square_new = 0.9 * square[...] + 0.1 * piece * piece
+        mean_new = 0.8 * mean[...] + 0.2 * low
+        square_new = 0.9 * square[...] + 0.1 * low * low
         mean_out[...] = mean_new
         square_out[...] = square_new
-        direction = (mean_new / jnp.sqrt(square_new)).astype(BF16)
-        out[:, :, at] = jnp.broadcast_to(direction, (count, *direction.shape))
+        directions.append(mean_new / jnp.sqrt(square_new))
+    out[...] = jnp.broadcast_to(folded(*directions).astype(BF16), out.shape)
 
 
 def sums_body(width_q, piece, out):
     x = piece[...].astype(F32)
     squares = jnp.sum(jnp.sum(x * x, axis=0), axis=0, keepdims=True)
+    at = squares.shape[1] - 2 * width_q
     half = (out.shape[0], out.shape[1] // 2, out.shape[2])
-    out[:, : half[1]] = jnp.broadcast_to(jnp.sum(squares[:, :width_q], keepdims=True)[None], half)
-    out[:, half[1] :] = jnp.broadcast_to(jnp.sum(squares[:, width_q:], keepdims=True)[None], half)
+    out[:, : half[1]] = jnp.broadcast_to(jnp.sum(squares[:, at:], keepdims=True)[None], half)
+    out[:, half[1] :] = jnp.broadcast_to(jnp.sum(squares[:, :at], keepdims=True)[None], half)
 
 
 def product_body(kept, piece, fq_own, fo_own, step_q, step_o, all_q_t, all_o):
@@ -161,17 +173,19 @@
     rows = rows_q + step_o.shape[0]
     count = kept.shape[1]
     rank = fq_own.shape[1]
-    whole = in_order(piece[...]).reshape(rank, -1)
-    step_q[...] = contract(fq_own[...], whole[:, :width_q], 1, 0)
-    step_o[...] = contract(fo_own[...], whole[:, width_q:], 1, 0)
+    direction_q, direction_o = (
+        x.reshape(rank, -1).astype(BF16) for x in unfolded(in_order(piece[...].astype(F32), DIRECTION), width_q)
+    )
+    step_q[...] = contract(fq_own[...], direction_q, 1, 0)
+    step_o[...] = contract(fo_own[...], direction_o, 1, 0)
     step_all_q = 0.0
     step_all_o = 0.0
     for core in range(2):
-        direction = whole[core * LANES : (core + 1) * LANES]
-        fq = in_order(kept[core, :, :rows_q]).reshape(count * rows_q, LANES)
-        fo = in_order(kept[core, :, rows_q:rows]).reshape(count * (rows - rows_q), LANES)
-        step_all_q = step_all_q + contract(fq, direction[:, :width_q], 1, 0)
-        step_all_o = step_all_o + contract(fo, direction[:, width_q:], 1, 0)
+        at = slice(core * LANES, (core + 1) * LANES)
+        fq = in_order(kept[core, :, :rows_q], FIRST).reshape(count * rows_q, LANES)
+        fo = in_order(kept[core, :, rows_q:rows], FIRST).reshape(count * (rows - rows_q), LANES)
+        step_all_q = step_all_q + contract(fq, direction_q[at], 1, 0)
+        step_all_o = step_all_o + contract(fo, direction_o[at], 1, 0)
     all_q_t[...] = step_all_q.T.astype(BF16)
     all_o[...] = step_all_o.astype(BF16)
 
@@ -181,7 +195,7 @@
     width_q = whole_q_t.shape[0]
     for k, ref in enumerate((w0, w1, w2, w3)):
         u = (y + (RING - k)) % RING
-        got = in_order(ref[...].astype(F32))
+        got = in_order(ref[...].astype(F32), FIRST)
         held_q[u // 2, :, u % 2] = got[:, 0:8]
         held_o[0, :, u] = got[:, 8:16]
         held_o[1, :, u] = got[:, 16:24]
@@ -244,7 +258,7 @@
             pltpu.SemaphoreType.DMA((count // RING,)),
         ),
     )
-    own = exchange(packed, "fs", exchange_order(count))
+    own = exchange(packed, "fs", exchange_order(count, FIRST))
     grad_q_t = contract(query_cot, latent_in, 0, 0).astype(BF16)
     grad_o = contract(attn_out, mix_cot, 0, 0).astype(BF16)
     other = lax.ppermute(own, "tp", [(i, i ^ 1) for i in range(columns)])
@@ -255,7 +269,7 @@
 
     (low,) = on_chip(
         functools.partial(low_body, inv_root, rows_q, rows),
-        [((count, rank // count, width), BF16, FAR)],
+        [((count, rank // count // 2, 2 * width), BF16, FAR)],
         near(own), near(other), near(grad_q_t), near(grad_o),
     )
     (kept,) = on_chip(
@@ -264,15 +278,15 @@
         near(own), near(other),
         scratch=(pltpu.SemaphoreType.DMA((2,)),),
     )
-    parts = exchange(low, "fs", exchange_order(count))
+    parts = exchange(low, "fs", exchange_order(count, LOW))
     of_q = (query_mean.shape, F32, FAR)
     of_o = (output_mean.shape, F32, FAR)
     mean_q, square_q, mean_o, square_o, joined = on_chip(
         moments_body,
-        [of_q, of_q, of_o, of_o, ((count, rank // count, width), BF16, FAR)],
+        [of_q, of_q, of_o, of_o, ((count, rank // count // 2, 2 * width), BF16, FAR)],
         near(parts), query_mean, query_square, output_mean, output_square, limit=SMALL,
     )
-    piece = exchange(joined, "fs", exchange_order(count))
+    piece = exchange(joined, "fs", exchange_order(count, DIRECTION))
     wholes = on_chip(
         assemble_body,
         [((width_q, rows_q * count), BF16, FAR), ((rows_o * count, width_o), BF16, FAR)],
@@ -307,7 +321,7 @@
             ((width_q, rows_q * count), BF16, FAR),
             ((rows_o * count, width_o), BF16, FAR),
         ],
-        *wholes, near(sums), *map(near, products), query_weight, output_weight,
+        *wholes, near(sums), *map(near, products), query_weight, output_weight, limit=24 * 2**20,
     )
     return (step_q, step_o, new_q, new_o, copy_q_t.T, copy_o, mean_q, square_q, mean_o, square_o)
 

time: 88.8 us -> 85.3 us (0.961)
  the two profiles are of different devices: /device:TPU:1 before, /device:TPU:2 now
where the time goes in v5:
time: 85.3 us; the launch traced here: 83.8 us
  starting transfers between devices  28.8 us (34%)
  blocking collectives  17.3 us (20%)
  waiting for transfers between devices  16.7 us (20%)
  Pallas kernels  11.4 us (13%)
  matrix products  7.66 us (9%)
  local copies, waits for them, and re-layouts  1.11 us (1%)
    all_to_all x3, starting transfers between devices, exchange(): lax.all_to_all(tiles, axis, split_axis=0, concat_axis=0, tiled=True, axis...  26.7 us
    all_to_all x1, blocking collectives, exchange(): lax.all_to_all(tiles, axis, split_axis=0, concat_axis=0, tiled=True, axis...  17.3 us
    all_to_all x3, waiting for transfers between devices, exchange(): lax.all_to_all(tiles, axis, split_axis=0, concat_axis=0, tiled=True, axis...  13.8 us
    pallas_call x8, Pallas kernels, on_chip(): pl.pallas_call(body, out_shape=tuple((pltpu.VMEM(s, d) if at == NEAR else...  11.4 us
    dot_general x2, matrix products, contract(): return lax.dot_general(left, right, dims, preferred_element_type=F32)  7.66 us
    ppermute x3, waiting for transfers between devices, on_device(): held.append(lax.ppermute(held[0], 'fs', pairs))  2.89 us
    ppermute x3, starting transfers between devices, on_device(): held.append(lax.ppermute(held[0], 'fs', pairs))  2.11 us
  transfers between devices with their start and end apart: 7, of which 4 were waited for; matrix products, arithmetic and copies ran while one was open for 9% of the time, Pallas kernels for 7%

profile of v5, /device:TPU:2, one launch (start us, length us, event | category | flops | bytes accessed | tf_op | source)
XLA Modules:
  0.0 83.8 jit_solution(10061317569735160619)
XLA Ops:
  0.6 0.0 copy-start
  0.7 1.8 %shard_map.195 = bf16[32,72,128]{2,1,0:T(8,128)(2,1)} custom-call(bf16[16,256]{1,0:T(8,128)(2,1)} %fq_own.1, bf16[32,256]{1,0:T(8,128)(2,1)} %fo_own.1, f32[16,192]{1,0:T(8,128)} %wq.3, f32[32,256]{1,0:T(8,128)} %wo.3), custom_call_target="tpu_custom_call" | custom-call | tf_op jit(solution)/shard_map/pallas_call | solution.py:41
  2.5 13.0 %all-to-all-start = ((bf16[32,72,128]{2,1,0:T(8,128)(2,1)}), bf16[32,72,128]{2,1,0:T(8,128)(2,1)S(1)}, u32[]{:S(2)}, u32[]{:S(2)}) async-start(bf16[32,72,128]{2,1,0:T(8,128)(2,1)} %shard_map.195), calls=%async_computation | async-start | bytes 1179648 | tf_op jit(solution)/shard_map/all_to_all | solution.py:21
  15.5 3.0 %convolution_convert_fusion.1.gq_t = bf16[192,512]{1,0:T(8,128)(2,1)S(1)} fusion(bf16[3072,192]{0,1:T(8,128)(2,1)} %param.13, bf16[3072,512]{1,0:T(8,128)(2,1)} %param.12), kind=kOutput, calls=%fused_computation.1 | convolution fusion | flops 604078080 | bytes 4521984 | tf_op jit(solution)/shard_map/dot_general | solution.py:28
  18.6 10.8 %all-to-all-done.own = bf16[32,72,128]{2,1,0:T(8,128)(2,1)S(1)} async-done(((bf16[32,72,128]{2,1,0:T(8,128)(2,1)}), bf16[32,72,128]{2,1,0:T(8,128)(2,1)S(1)}, u32[]{:S(2)}, u32[]{:S(2)}) %all-to-all-start) | async-done | bytes 589856 | tf_op jit(solution)/shard_map/all_to_all | solution.py:21
  29.3 0.0 collective-permute-start.3
  29.4 4.6 %convolution_convert_fusion.go = bf16[1024,256]{1,0:T(8,128)(2,1)S(1)} fusion(bf16[3072,1024]{1,0:T(8,128)(2,1)} %param.14, bf16[3072,256]{1,0:T(8,128)(2,1)S(1)} %copy-done), kind=kOutput, calls=%fused_computation | convolution fusion | flops 1610874880 | bytes 8388608 | tf_op jit(solution)/shard_map/dot_general | solution.py:28
  34.0 0.0 copy-start.5
  34.0 0.0 copy-start.6
  34.0 0.0 copy-start.7
  34.0 0.0 copy-start.8
  34.0 1.1 %shard_map.197 = bf16[32,4,896]{2,1,0:T(4,128)(2,1)} custom-call(bf16[32,72,128]{2,1,0:T(8,128)(2,1)S(1)} %all-to-all-done.own, bf16[32,72,128]{2,1,0:T(8,128)(2,1)S(1)} %collective-permute-done.3.other, bf16[192,512]{1,0:T(8,128)(2,1)S(1)} %convolution_convert_fusion.1.gq_t, bf16[1024,256]{1,0:T(8,128)(2,1)S(1)} %convolution_convert_fusion.go), custom_call_target="tpu_custom_call" | custom-call | tf_op jit(solution)/shard_map/pallas_call | solution.py:41
  35.2 17.3 %all_to_all.20.parts = bf16[32,4,896]{2,1,0:T(4,128)(2,1)S(1)} all-to-all(bf16[32,4,896]{2,1,0:T(4,128)(2,1)} %shard_map.197), channel_id=1, replica_groups={{176,184,160,168,208,216,192,200,240,248,224,232,16,24,0,8,48,56,32,40,..., dimensions={0} | all-to-all | bytes 458752 | tf_op jit(solution)/shard_map/all_to_all | solution.py:21
  52.5 0.9 %shard_map.198 = (f32[8,192]{1,0:T(8,128)}, f32[8,192]{1,0:T(8,128)}, f32[8,256]{1,0:T(8,128)}, f32[8,256]{1,0:T(8,128)}, bf16[32,4,896]{2,1,0:T(4,128)(2,1)}) custom-call(bf16[32,4,896]{2,1,0:T(4,128)(2,1)S(1)} %all_to_all.20.parts, f32[8,192]{1,0:T(8,128)S(1)} %copy-done.5, f32[8,192]{1,0:T(8,128)S(1)} %copy-done.6, f32[8,256]{1,0:T(8,128)S(1)} %copy-done.7, ...), custom_call_target="tpu_custom_call" | custom-call | tf_op jit(solution)/shard_map/pallas_call | solution.py:41
  53.4 10.0 %all-to-all-start.2 = ((bf16[32,4,896]{2,1,0:T(4,128)(2,1)}), bf16[32,4,896]{2,1,0:T(4,128)(2,1)S(1)}, u32[]{:S(2)}, u32[]{:S(2)}) async-start(bf16[32,4,896]{2,1,0:T(4,128)(2,1)} %get-tuple-element.29), calls=%async_computation.2 | async-start | bytes 458752 | tf_op jit(solution)/shard_map/all_to_all | solution.py:21
  63.5 0.0 copy-start.9
  63.5 0.6 collective-permute-start.2
  64.1 1.5 %collective-permute-start.1 = (bf16[32,24,128]{2,1,0:T(8,128)(2,1)S(1)}, bf16[32,24,128]{2,1,0:T(8,128)(2,1)}, u32[]{:S(2)}, u32[]{:S(2)}) collective-permute-start(bf16[32,24,128]{2,1,0:T(8,128)(2,1)S(1)} %slice.4.w0), channel_id=1, source_target_pairs={{0,16},{8,24},{16,0},{24,8},{32,48},{40,56},{48,32},{56,40},{64,80... | collective-permute-start | bytes 589832 | tf_op jit(solution)/shard_map/ppermute | solution.py:268
  65.6 0.0 collective-permute-start
  65.6 3.0 %all-to-all-done.2.piece = bf16[32,4,896]{2,1,0:T(4,128)(2,1)S(1)} async-done(((bf16[32,4,896]{2,1,0:T(4,128)(2,1)}), bf16[32,4,896]{2,1,0:T(4,128)(2,1)S(1)}, u32[]{:S(2)}, u32[]{:S(2)}) %all-to-all-start.2) | async-done | bytes 229408 | tf_op jit(solution)/shard_map/all_to_all | solution.py:21
  68.6 0.9 %shard_map.199 = f32[8,8,128]{2,1,0:T(8,128)} custom-call(bf16[32,4,896]{2,1,0:T(4,128)(2,1)S(1)} %all-to-all-done.2.piece), custom_call_target="tpu_custom_call" | custom-call | tf_op jit(solution)/shard_map/pallas_call | solution.py:41
  69.5 3.7 %all-to-all-start.3 = ((f32[8,8,128]{2,1,0:T(8,128)}), f32[8,8,128]{2,1,0:T(8,128)S(1)}, u32[]{:S(2)}, u32[]{:S(2)}) async-start(f32[8,8,128]{2,1,0:T(8,128)} %shard_map.199), calls=%async_computation.3 | async-start | bytes 65536 | tf_op jit(solution)/shard_map/all_to_all | solution.py:21
  73.2 0.0 collective-permute-done.2.w3
  73.2 0.4 collective-permute-done.1.w2
  73.5 2.5 %collective-permute-done.w1 = bf16[32,24,128]{2,1,0:T(8,128)(2,1)} collective-permute-done((bf16[32,24,128]{2,1,0:T(8,128)(2,1)S(1)}, bf16[32,24,128]{2,1,0:T(8,128)(2,1)}, u32[]{:S(2)}, u32[]{:S(2)}) %collective-permute-start) | collective-permute-done | bytes 196640 | tf_op jit(solution)/shard_map/ppermute | solution.py:268
  76.1 2.4 %shard_map.196 = (bf16[192,512]{1,0:T(8,128)(2,1)}, bf16[1024,256]{1,0:T(8,128)(2,1)}) custom-call(bf16[32,24,128]{2,1,0:T(8,128)(2,1)} %copy-done.9, bf16[32,24,128]{2,1,0:T(8,128)(2,1)} %collective-permute-done.w1, bf16[32,24,128]{2,1,0:T(8,128)(2,1)} %collective-permute-done.1.w2, bf16[32,24,128]{2,1,0:T(8,128)(2,1)} %copy-done.10), custom_call_target="tpu_custom_call" | custom-call | tf_op jit(solution)/shard_map/pallas_call | solution.py:41
  78.4 1.1 %shard_map.200.kept = bf16[2,32,72,128]{3,2,1,0:T(8,128)(2,1)} custom-call(bf16[32,72,128]{2,1,0:T(8,128)(2,1)S(1)} %all-to-all-done.own, bf16[32,72,128]{2,1,0:T(8,128)(2,1)S(1)} %collective-permute-done.3.other), custom_call_target="tpu_custom_call" | custom-call | tf_op jit(solution)/shard_map/pallas_call | solution.py:41
  79.5 1.9 %shard_map.201 = (f32[16,192]{1,0:T(8,128)S(1)}, f32[32,256]{1,0:T(8,128)S(1)}, bf16[192,512]{1,0:T(8,128)(2,1)S(1)}, bf16[1024,256]{1,0:T(8,128)(2,1)S(1)}) custom-call(bf16[2,32,72,128]{3,2,1,0:T(8,128)(2,1)} %shard_map.200.kept, bf16[32,4,896]{2,1,0:T(4,128)(2,1)S(1)} %all-to-all-done.2.piece, bf16[16,256]{1,0:T(8,128)(2,1)} %fq_own.1, bf16[32,256]{1,0:T(8,128)(2,1)} %fo_own.1), custom_call_target="tpu_custom_call" | custom-call | tf_op jit(solution)/shard_map/pallas_call | solution.py:41
  81.5 0.0 all-to-all-done.3.sums
  81.5 0.0 copy-start.1
  81.5 1.0 %copy-done.1 = bf16[1024,256]{1,0:T(8,128)(2,1)S(1)} copy-done((bf16[1024,256]{1,0:T(8,128)(2,1)S(1)}, bf16[1024,256]{1,0:T(8,128)(2,1)}, u32[]{:S(2)}) %copy-start.1) | copy-done | bytes 524312
  82.5 1.3 %shard_map.202 = (f32[16,192]{1,0:T(8,128)}, f32[32,256]{1,0:T(8,128)}, f32[16,192]{1,0:T(8,128)}, f32[32,256]{1,0:T(8,128)}, bf16[192,512]{1,0:T(8,128)(2,1)}, /*index=5*/bf16[1024,256]{1,0:T(8,128)(2,1)}) custom-call(bf16[192,512]{1,0:T(8,128)(2,1)S(1)} %copy-done.2, bf16[1024,256]{1,0:T(8,128)(2,1)S(1)} %copy-done.1, ...), custom_call_target="tpu_custom_call" | custom-call | tf_op jit(solution)/shard_map/pallas_call | solution.py:41
  (16 shorter events, 0.1 us)
Async XLA Ops:
  0.6 28.7 %copy-start = (bf16[3072,256]{1,0:T(8,128)(2,1)S(1)}, bf16[3072,256]{1,0:T(8,128)(2,1)}, u32[]{:S(2)}) copy-start(bf16[3072,256]{1,0:T(8,128)(2,1)} %param.15) | copy-start | bytes 4718596
  2.5 26.8 %all-to-all-start = ((bf16[32,72,128]{2,1,0:T(8,128)(2,1)}), bf16[32,72,128]{2,1,0:T(8,128)(2,1)S(1)}, u32[]{:S(2)}, u32[]{:S(2)}) async-start(bf16[32,72,128]{2,1,0:T(8,128)(2,1)} %shard_map.195), calls=%async_computation | async-start | bytes 1179648 | tf_op jit(solution)/shard_map/all_to_all | solution.py:21
  29.3 4.7 %collective-permute-start.3 = (bf16[32,72,128]{2,1,0:T(8,128)(2,1)S(1)}, bf16[32,72,128]{2,1,0:T(8,128)(2,1)S(1)}, u32[]{:S(2)}, u32[]{:S(2)}) collective-permute-start(bf16[32,72,128]{2,1,0:T(8,128)(2,1)S(1)} %all-to-all-done.own), channel_id=1, source_target_pairs={{0,1},{1,0},{2,3},{3,2},{4,5},{5,4},{6,7},{7,6},{8,9},{9,8},{10,11... | collective-permute-start | bytes 1769480 | tf_op jit(solution)/shard_map/ppermute | solution.py:264
  34.0 18.5 %copy-start.5 = (f32[8,192]{1,0:T(8,128)S(1)}, f32[8,192]{1,0:T(8,128)}, u32[]{:S(2)}) copy-start(f32[8,192]{1,0:T(8,128)} %mq.1) | copy-start | bytes 18436
  34.0 18.5 %copy-start.6 = (f32[8,192]{1,0:T(8,128)S(1)}, f32[8,192]{1,0:T(8,128)}, u32[]{:S(2)}) copy-start(f32[8,192]{1,0:T(8,128)} %sq.1) | copy-start | bytes 18436
  34.0 18.5 %copy-start.7 = (f32[8,256]{1,0:T(8,128)S(1)}, f32[8,256]{1,0:T(8,128)}, u32[]{:S(2)}) copy-start(f32[8,256]{1,0:T(8,128)} %mo.1) | copy-start | bytes 24580
  34.0 18.5 %copy-start.8 = (f32[8,256]{1,0:T(8,128)S(1)}, f32[8,256]{1,0:T(8,128)}, u32[]{:S(2)}) copy-start(f32[8,256]{1,0:T(8,128)} %so.1) | copy-start | bytes 24580
  53.4 15.2 %all-to-all-start.2 = ((bf16[32,4,896]{2,1,0:T(4,128)(2,1)}), bf16[32,4,896]{2,1,0:T(4,128)(2,1)S(1)}, u32[]{:S(2)}, u32[]{:S(2)}) async-start(bf16[32,4,896]{2,1,0:T(4,128)(2,1)} %get-tuple-element.29), calls=%async_computation.2 | async-start | bytes 458752 | tf_op jit(solution)/shard_map/all_to_all | solution.py:21
  63.5 12.6 %copy-start.9 = (bf16[32,24,128]{2,1,0:T(8,128)(2,1)}, bf16[32,24,128]{2,1,0:T(8,128)(2,1)S(1)}, u32[]{:S(2)}) copy-start(bf16[32,24,128]{2,1,0:T(8,128)(2,1)S(1)} %slice.4.w0) | copy-start | bytes 589828
  63.5 9.7 %collective-permute-start.2 = (bf16[32,24,128]{2,1,0:T(8,128)(2,1)S(1)}, bf16[32,24,128]{2,1,0:T(8,128)(2,1)S(1)}, u32[]{:S(2)}, u32[]{:S(2)}) collective-permute-start(bf16[32,24,128]{2,1,0:T(8,128)(2,1)S(1)} %slice.4.w0), channel_id=1, source_target_pairs={{0,24},{8,0},{16,8},{24,16},{32,56},{40,32},{48,40},{56,48},{64,88... | collective-permute-start | bytes 589832 | tf_op jit(solution)/shard_map/ppermute | solution.py:268
  64.1 9.4 %collective-permute-start.1 = (bf16[32,24,128]{2,1,0:T(8,128)(2,1)S(1)}, bf16[32,24,128]{2,1,0:T(8,128)(2,1)}, u32[]{:S(2)}, u32[]{:S(2)}) collective-permute-start(bf16[32,24,128]{2,1,0:T(8,128)(2,1)S(1)} %slice.4.w0), channel_id=1, source_target_pairs={{0,16},{8,24},{16,0},{24,8},{32,48},{40,56},{48,32},{56,40},{64,80... | collective-permute-start | bytes 589832 | tf_op jit(solution)/shard_map/ppermute | solution.py:268
  65.6 10.5 %collective-permute-start = (bf16[32,24,128]{2,1,0:T(8,128)(2,1)S(1)}, bf16[32,24,128]{2,1,0:T(8,128)(2,1)}, u32[]{:S(2)}, u32[]{:S(2)}) collective-permute-start(bf16[32,24,128]{2,1,0:T(8,128)(2,1)S(1)} %slice.4.w0), channel_id=1, source_target_pairs={{0,8},{8,16},{16,24},{24,0},{32,40},{40,48},{48,56},{56,32},{64,72... | collective-permute-start | bytes 589832 | tf_op jit(solution)/shard_map/ppermute | solution.py:268
  69.5 12.0 %all-to-all-start.3 = ((f32[8,8,128]{2,1,0:T(8,128)}), f32[8,8,128]{2,1,0:T(8,128)S(1)}, u32[]{:S(2)}, u32[]{:S(2)}) async-start(f32[8,8,128]{2,1,0:T(8,128)} %shard_map.199), calls=%async_computation.3 | async-start | bytes 65536 | tf_op jit(solution)/shard_map/all_to_all | solution.py:21
  73.2 2.9 %copy-start.10 = (bf16[32,24,128]{2,1,0:T(8,128)(2,1)}, bf16[32,24,128]{2,1,0:T(8,128)(2,1)S(1)}, u32[]{:S(2)}) copy-start(bf16[32,24,128]{2,1,0:T(8,128)(2,1)S(1)} %collective-permute-done.2.w3) | copy-start | bytes 589828
  78.4 3.0 %copy-start.2 = (bf16[192,512]{1,0:T(8,128)(2,1)S(1)}, bf16[192,512]{1,0:T(8,128)(2,1)}, u32[]{:S(2)}) copy-start(bf16[192,512]{1,0:T(8,128)(2,1)} %get-tuple-element.27.whole_q_t) | copy-start | bytes 589828
  78.4 3.0 %copy-start.3 = (f32[32,256]{1,0:T(8,128)S(1)}, f32[32,256]{1,0:T(8,128)}, u32[]{:S(2)}) copy-start(f32[32,256]{1,0:T(8,128)} %wo.3) | copy-start | bytes 98308
  78.4 3.1 %copy-start.4 = (f32[16,192]{1,0:T(8,128)S(1)}, f32[16,192]{1,0:T(8,128)}, u32[]{:S(2)}) copy-start(f32[16,192]{1,0:T(8,128)} %wq.3) | copy-start | bytes 36868
  81.5 1.0 %copy-start.1 = (bf16[1024,256]{1,0:T(8,128)(2,1)S(1)}, bf16[1024,256]{1,0:T(8,128)(2,1)}, u32[]{:S(2)}) copy-start(bf16[1024,256]{1,0:T(8,128)(2,1)} %get-tuple-element.28.whole_o) | copy-start | bytes 1572868

commit v6 on v5

--- a/solution.py
+++ b/solution.py
@@ -35,13 +35,13 @@
 FAR, NEAR, BY_HAND = "far", "near", "by hand"
 
 
-def on_chip(body, outs, *args, scratch=(), limit=None):
+def on_chip(body, outs, *args, scratch=(), limit=None, by_hand=0):
     vmem = pl.BlockSpec(memory_space=pltpu.VMEM)
     hand = pl.BlockSpec(memory_space=pl.ANY)
     return pl.pallas_call(
         body,
         out_shape=tuple(pltpu.VMEM(s, d) if at == NEAR else jax.ShapeDtypeStruct(s, d) for s, d, at in outs),
-        in_specs=[vmem] * len(args),
+        in_specs=[hand] * by_hand + [vmem] * (len(args) - by_hand),
         out_specs=tuple(hand if at == BY_HAND else vmem for _, _, at in outs),
         scratch_shapes=list(scratch),
         compiler_params=pltpu.CompilerParams(vmem_limit_bytes=limit),
@@ -85,24 +85,33 @@
     return q, o
 
 
-def pack_body(fq, fo, wq, wo, out, tiles, sems):
+def pack_body(fq, fo, wq, wo, out, tiles, got_q, got_o, reads, sems):
     count = out.shape[0]
     core = lax.axis_index("tp") % 2
     rows_q, rows_o = fq.shape[0], fo.shape[0]
     rows = rows_q + rows_o
     width_q = wq.shape[1]
+    weights = [pltpu.make_async_copy(wq, got_q, reads.at[0]), pltpu.make_async_copy(wo, got_o, reads.at[1])]
+    columns = pl.ds(pl.multiple_of(core * LANES, LANES), LANES)
+    factors = []
     for y in range(RING):
-        for f, at in ((fq, 0), (fo, rows_q)):
-            left, right = halves(f[...])
-            half = jnp.where(core == 0, left.astype(F32), right.astype(F32)).astype(BF16)
-            tiles[y, at : at + f.shape[0]] = half
+        for k, (f, at) in enumerate(((fq, 0), (fo, rows_q))):
+            to = tiles.at[y, at : at + f.shape[0]]
+            factors.append(pltpu.make_async_copy(f.at[:, columns], to, reads.at[2 + 2 * y + k]))
+    for copy in weights + factors:
+        copy.start()
+    for copy in weights:
+        copy.wait()
+    for y in range(RING):
         to = (y + FIRST[1]) % RING
         row, col = to % 2, to // 2
-        part = wq[8 * row : 8 * row + 8, col * LANES : min(width_q, (col + 1) * LANES)]
+        part = got_q[8 * row : 8 * row + 8, col * LANES : min(width_q, (col + 1) * LANES)]
         if part.shape[1] < LANES:
             part = jnp.concatenate([part, jnp.zeros((8, LANES - part.shape[1]), F32)], axis=1)
-        left, right = halves(wo[8 * to : 8 * to + 8, :])
+        left, right = halves(got_o[8 * to : 8 * to + 8, :])
         tiles[y, rows:] = jnp.concatenate([part, left, right], axis=0).astype(BF16)
+    for copy in factors:
+        copy.wait()
     copies = [
         pltpu.make_async_copy(tiles, out.at[pl.ds(z * RING, RING)], sems.at[z])
         for z in range(count // RING)
@@ -255,8 +264,12 @@
         query_factor, output_factor, query_weight, output_weight,
         scratch=(
             pltpu.VMEM((RING, rows + quarter, LANES), BF16),
+            pltpu.VMEM(query_weight.shape, F32),
+            pltpu.VMEM(output_weight.shape, F32),
+            pltpu.SemaphoreType.DMA((2 + 2 * RING,)),
             pltpu.SemaphoreType.DMA((count // RING,)),
         ),
+        by_hand=4,
     )
     own = exchange(packed, "fs", exchange_order(count, FIRST))
     grad_q_t = contract(query_cot, latent_in, 0, 0).astype(BF16)

time: 85.3 us -> 85.4 us (level)
  no operation moved by 1% of the time
where the time goes in v6:
time: 85.4 us; the launch traced here: 83.9 us
  starting transfers between devices  28.8 us (34%)
  blocking collectives  17.3 us (20%)
  waiting for transfers between devices  16.7 us (20%)
  Pallas kernels  11.5 us (13%)
  matrix products  7.64 us (9%)
  local copies, waits for them, and re-layouts  1.11 us (1%)
    all_to_all x3, starting transfers between devices, exchange(): lax.all_to_all(tiles, axis, split_axis=0, concat_axis=0, tiled=True, axis...  26.7 us
    all_to_all x1, blocking collectives, exchange(): lax.all_to_all(tiles, axis, split_axis=0, concat_axis=0, tiled=True, axis...  17.3 us
    all_to_all x3, waiting for transfers between devices, exchange(): lax.all_to_all(tiles, axis, split_axis=0, concat_axis=0, tiled=True, axis...  13.8 us
    pallas_call x8, Pallas kernels, on_chip(): pl.pallas_call(body, out_shape=tuple((pltpu.VMEM(s, d) if at == NEAR else...  11.5 us
    dot_general x2, matrix products, contract(): return lax.dot_general(left, right, dims, preferred_element_type=F32)  7.64 us
    ppermute x3, waiting for transfers between devices, on_device(): held.append(lax.ppermute(held[0], 'fs', pairs))  2.89 us
    ppermute x3, starting transfers between devices, on_device(): held.append(lax.ppermute(held[0], 'fs', pairs))  2.11 us
  transfers between devices with their start and end apart: 7, of which 4 were waited for; matrix products, arithmetic and copies ran while one was open for 9% of the time, Pallas kernels for 7%

profile of v6, /device:TPU:2, one launch (start us, length us, event | category | flops | bytes accessed | tf_op | source)
XLA Modules:
  0.0 83.9 jit_solution(1839908132428567325)
XLA Ops:
  0.6 0.0 copy-start
  0.7 1.9 %shard_map.195 = bf16[32,72,128]{2,1,0:T(8,128)(2,1)} custom-call(bf16[16,256]{1,0:T(8,128)(2,1)} %fq_own.1, bf16[32,256]{1,0:T(8,128)(2,1)} %fo_own.1, f32[16,192]{1,0:T(8,128)} %wq.3, f32[32,256]{1,0:T(8,128)} %wo.3), custom_call_target="tpu_custom_call" | custom-call | tf_op jit(solution)/shard_map/pallas_call | solution.py:41
  2.6 13.0 %all-to-all-start = ((bf16[32,72,128]{2,1,0:T(8,128)(2,1)}), bf16[32,72,128]{2,1,0:T(8,128)(2,1)S(1)}, u32[]{:S(2)}, u32[]{:S(2)}) async-start(bf16[32,72,128]{2,1,0:T(8,128)(2,1)} %shard_map.195), calls=%async_computation | async-start | bytes 1179648 | tf_op jit(solution)/shard_map/all_to_all | solution.py:21
  15.6 3.0 %convolution_convert_fusion.1.gq_t = bf16[192,512]{1,0:T(8,128)(2,1)S(1)} fusion(bf16[3072,192]{0,1:T(8,128)(2,1)} %param.13, bf16[3072,512]{1,0:T(8,128)(2,1)} %param.12), kind=kOutput, calls=%fused_computation.1 | convolution fusion | flops 604078080 | bytes 4521984 | tf_op jit(solution)/shard_map/dot_general | solution.py:28
  18.7 10.8 %all-to-all-done.own = bf16[32,72,128]{2,1,0:T(8,128)(2,1)S(1)} async-done(((bf16[32,72,128]{2,1,0:T(8,128)(2,1)}), bf16[32,72,128]{2,1,0:T(8,128)(2,1)S(1)}, u32[]{:S(2)}, u32[]{:S(2)}) %all-to-all-start) | async-done | bytes 589856 | tf_op jit(solution)/shard_map/all_to_all | solution.py:21
  29.4 0.0 collective-permute-start.3
  29.4 4.6 %convolution_convert_fusion.go = bf16[1024,256]{1,0:T(8,128)(2,1)S(1)} fusion(bf16[3072,1024]{1,0:T(8,128)(2,1)} %param.14, bf16[3072,256]{1,0:T(8,128)(2,1)S(1)} %copy-done), kind=kOutput, calls=%fused_computation | convolution fusion | flops 1610874880 | bytes 8388608 | tf_op jit(solution)/shard_map/dot_general | solution.py:28
  34.1 0.0 copy-start.5
  34.1 0.0 copy-start.6
  34.1 0.0 copy-start.7
  34.1 0.0 copy-start.8
  34.1 0.0 collective-permute-done.3.other
  34.1 1.2 %shard_map.197 = bf16[32,4,896]{2,1,0:T(4,128)(2,1)} custom-call(bf16[32,72,128]{2,1,0:T(8,128)(2,1)S(1)} %all-to-all-done.own, bf16[32,72,128]{2,1,0:T(8,128)(2,1)S(1)} %collective-permute-done.3.other, bf16[192,512]{1,0:T(8,128)(2,1)S(1)} %convolution_convert_fusion.1.gq_t, bf16[1024,256]{1,0:T(8,128)(2,1)S(1)} %convolution_convert_fusion.go), custom_call_target="tpu_custom_call" | custom-call | tf_op jit(solution)/shard_map/pallas_call | solution.py:41
  35.3 17.3 %all_to_all.20.parts = bf16[32,4,896]{2,1,0:T(4,128)(2,1)S(1)} all-to-all(bf16[32,4,896]{2,1,0:T(4,128)(2,1)} %shard_map.197), channel_id=1, replica_groups={{176,184,160,168,208,216,192,200,240,248,224,232,16,24,0,8,48,56,32,40,..., dimensions={0} | all-to-all | bytes 458752 | tf_op jit(solution)/shard_map/all_to_all | solution.py:21
  52.6 0.9 %shard_map.198 = (f32[8,192]{1,0:T(8,128)}, f32[8,192]{1,0:T(8,128)}, f32[8,256]{1,0:T(8,128)}, f32[8,256]{1,0:T(8,128)}, bf16[32,4,896]{2,1,0:T(4,128)(2,1)}) custom-call(bf16[32,4,896]{2,1,0:T(4,128)(2,1)S(1)} %all_to_all.20.parts, f32[8,192]{1,0:T(8,128)S(1)} %copy-done.5, f32[8,192]{1,0:T(8,128)S(1)} %copy-done.6, f32[8,256]{1,0:T(8,128)S(1)} %copy-done.7, ...), custom_call_target="tpu_custom_call" | custom-call | tf_op jit(solution)/shard_map/pallas_call | solution.py:41
  53.5 10.0 %all-to-all-start.2 = ((bf16[32,4,896]{2,1,0:T(4,128)(2,1)}), bf16[32,4,896]{2,1,0:T(4,128)(2,1)S(1)}, u32[]{:S(2)}, u32[]{:S(2)}) async-start(bf16[32,4,896]{2,1,0:T(4,128)(2,1)} %get-tuple-element.29), calls=%async_computation.2 | async-start | bytes 458752 | tf_op jit(solution)/shard_map/all_to_all | solution.py:21
  63.6 0.0 copy-start.9
  63.6 0.6 collective-permute-start.2
  64.2 1.5 %collective-permute-start.1 = (bf16[32,24,128]{2,1,0:T(8,128)(2,1)S(1)}, bf16[32,24,128]{2,1,0:T(8,128)(2,1)}, u32[]{:S(2)}, u32[]{:S(2)}) collective-permute-start(bf16[32,24,128]{2,1,0:T(8,128)(2,1)S(1)} %slice.4.w0), channel_id=1, source_target_pairs={{0,16},{8,24},{16,0},{24,8},{32,48},{40,56},{48,32},{56,40},{64,80... | collective-permute-start | bytes 589832 | tf_op jit(solution)/shard_map/ppermute | solution.py:281
  65.7 0.0 collective-permute-start
  65.7 3.0 %all-to-all-done.2.piece = bf16[32,4,896]{2,1,0:T(4,128)(2,1)S(1)} async-done(((bf16[32,4,896]{2,1,0:T(4,128)(2,1)}), bf16[32,4,896]{2,1,0:T(4,128)(2,1)S(1)}, u32[]{:S(2)}, u32[]{:S(2)}) %all-to-all-start.2) | async-done | bytes 229408 | tf_op jit(solution)/shard_map/all_to_all | solution.py:21
  68.7 0.9 %shard_map.199 = f32[8,8,128]{2,1,0:T(8,128)} custom-call(bf16[32,4,896]{2,1,0:T(4,128)(2,1)S(1)} %all-to-all-done.2.piece), custom_call_target="tpu_custom_call" | custom-call | tf_op jit(solution)/shard_map/pallas_call | solution.py:41
  69.5 3.7 %all-to-all-start.3 = ((f32[8,8,128]{2,1,0:T(8,128)}), f32[8,8,128]{2,1,0:T(8,128)S(1)}, u32[]{:S(2)}, u32[]{:S(2)}) async-start(f32[8,8,128]{2,1,0:T(8,128)} %shard_map.199), calls=%async_computation.3 | async-start | bytes 65536 | tf_op jit(solution)/shard_map/all_to_all | solution.py:21
  73.2 0.0 collective-permute-done.2.w3
  73.2 0.4 collective-permute-done.1.w2
  73.6 2.5 %collective-permute-done.w1 = bf16[32,24,128]{2,1,0:T(8,128)(2,1)} collective-permute-done((bf16[32,24,128]{2,1,0:T(8,128)(2,1)S(1)}, bf16[32,24,128]{2,1,0:T(8,128)(2,1)}, u32[]{:S(2)}, u32[]{:S(2)}) %collective-permute-start) | collective-permute-done | bytes 196640 | tf_op jit(solution)/shard_map/ppermute | solution.py:281
  76.1 2.4 %shard_map.196 = (bf16[192,512]{1,0:T(8,128)(2,1)}, bf16[1024,256]{1,0:T(8,128)(2,1)}) custom-call(bf16[32,24,128]{2,1,0:T(8,128)(2,1)} %copy-done.9, bf16[32,24,128]{2,1,0:T(8,128)(2,1)} %collective-permute-done.w1, bf16[32,24,128]{2,1,0:T(8,128)(2,1)} %collective-permute-done.1.w2, bf16[32,24,128]{2,1,0:T(8,128)(2,1)} %copy-done.10), custom_call_target="tpu_custom_call" | custom-call | tf_op jit(solution)/shard_map/pallas_call | solution.py:41
  78.5 1.1 %shard_map.200.kept = bf16[2,32,72,128]{3,2,1,0:T(8,128)(2,1)} custom-call(bf16[32,72,128]{2,1,0:T(8,128)(2,1)S(1)} %all-to-all-done.own, bf16[32,72,128]{2,1,0:T(8,128)(2,1)S(1)} %collective-permute-done.3.other), custom_call_target="tpu_custom_call" | custom-call | tf_op jit(solution)/shard_map/pallas_call | solution.py:41
  79.6 1.9 %shard_map.201 = (f32[16,192]{1,0:T(8,128)S(1)}, f32[32,256]{1,0:T(8,128)S(1)}, bf16[192,512]{1,0:T(8,128)(2,1)S(1)}, bf16[1024,256]{1,0:T(8,128)(2,1)S(1)}) custom-call(bf16[2,32,72,128]{3,2,1,0:T(8,128)(2,1)} %shard_map.200.kept, bf16[32,4,896]{2,1,0:T(4,128)(2,1)S(1)} %all-to-all-done.2.piece, bf16[16,256]{1,0:T(8,128)(2,1)} %fq_own.1, bf16[32,256]{1,0:T(8,128)(2,1)} %fo_own.1), custom_call_target="tpu_custom_call" | custom-call | tf_op jit(solution)/shard_map/pallas_call | solution.py:41
  81.6 0.0 copy-start.1
  81.6 1.0 %copy-done.1 = bf16[1024,256]{1,0:T(8,128)(2,1)S(1)} copy-done((bf16[1024,256]{1,0:T(8,128)(2,1)S(1)}, bf16[1024,256]{1,0:T(8,128)(2,1)}, u32[]{:S(2)}) %copy-start.1) | copy-done | bytes 524312
  82.6 1.3 %shard_map.202 = (f32[16,192]{1,0:T(8,128)}, f32[32,256]{1,0:T(8,128)}, f32[16,192]{1,0:T(8,128)}, f32[32,256]{1,0:T(8,128)}, bf16[192,512]{1,0:T(8,128)(2,1)}, /*index=5*/bf16[1024,256]{1,0:T(8,128)(2,1)}) custom-call(bf16[192,512]{1,0:T(8,128)(2,1)S(1)} %copy-done.2, bf16[1024,256]{1,0:T(8,128)(2,1)S(1)} %copy-done.1, ...), custom_call_target="tpu_custom_call" | custom-call | tf_op jit(solution)/shard_map/pallas_call | solution.py:41
  (16 shorter events, 0.1 us)
Async XLA Ops:
  0.6 28.8 %copy-start = (bf16[3072,256]{1,0:T(8,128)(2,1)S(1)}, bf16[3072,256]{1,0:T(8,128)(2,1)}, u32[]{:S(2)}) copy-start(bf16[3072,256]{1,0:T(8,128)(2,1)} %param.15) | copy-start | bytes 4718596
  2.6 26.8 %all-to-all-start = ((bf16[32,72,128]{2,1,0:T(8,128)(2,1)}), bf16[32,72,128]{2,1,0:T(8,128)(2,1)S(1)}, u32[]{:S(2)}, u32[]{:S(2)}) async-start(bf16[32,72,128]{2,1,0:T(8,128)(2,1)} %shard_map.195), calls=%async_computation | async-start | bytes 1179648 | tf_op jit(solution)/shard_map/all_to_all | solution.py:21
  29.4 4.7 %collective-permute-start.3 = (bf16[32,72,128]{2,1,0:T(8,128)(2,1)S(1)}, bf16[32,72,128]{2,1,0:T(8,128)(2,1)S(1)}, u32[]{:S(2)}, u32[]{:S(2)}) collective-permute-start(bf16[32,72,128]{2,1,0:T(8,128)(2,1)S(1)} %all-to-all-done.own), channel_id=1, source_target_pairs={{0,1},{1,0},{2,3},{3,2},{4,5},{5,4},{6,7},{7,6},{8,9},{9,8},{10,11... | collective-permute-start | bytes 1769480 | tf_op jit(solution)/shard_map/ppermute | solution.py:277
  34.1 18.5 %copy-start.5 = (f32[8,192]{1,0:T(8,128)S(1)}, f32[8,192]{1,0:T(8,128)}, u32[]{:S(2)}) copy-start(f32[8,192]{1,0:T(8,128)} %mq.1) | copy-start | bytes 18436
  34.1 18.5 %copy-start.6 = (f32[8,192]{1,0:T(8,128)S(1)}, f32[8,192]{1,0:T(8,128)}, u32[]{:S(2)}) copy-start(f32[8,192]{1,0:T(8,128)} %sq.1) | copy-start | bytes 18436
  34.1 18.5 %copy-start.7 = (f32[8,256]{1,0:T(8,128)S(1)}, f32[8,256]{1,0:T(8,128)}, u32[]{:S(2)}) copy-start(f32[8,256]{1,0:T(8,128)} %mo.1) | copy-start | bytes 24580
  34.1 18.5 %copy-start.8 = (f32[8,256]{1,0:T(8,128)S(1)}, f32[8,256]{1,0:T(8,128)}, u32[]{:S(2)}) copy-start(f32[8,256]{1,0:T(8,128)} %so.1) | copy-start | bytes 24580
  53.5 15.2 %all-to-all-start.2 = ((bf16[32,4,896]{2,1,0:T(4,128)(2,1)}), bf16[32,4,896]{2,1,0:T(4,128)(2,1)S(1)}, u32[]{:S(2)}, u32[]{:S(2)}) async-start(bf16[32,4,896]{2,1,0:T(4,128)(2,1)} %get-tuple-element.29), calls=%async_computation.2 | async-start | bytes 458752 | tf_op jit(solution)/shard_map/all_to_all | solution.py:21
  63.6 12.6 %copy-start.9 = (bf16[32,24,128]{2,1,0:T(8,128)(2,1)}, bf16[32,24,128]{2,1,0:T(8,128)(2,1)S(1)}, u32[]{:S(2)}) copy-start(bf16[32,24,128]{2,1,0:T(8,128)(2,1)S(1)} %slice.4.w0) | copy-start | bytes 589828
  63.6 9.7 %collective-permute-start.2 = (bf16[32,24,128]{2,1,0:T(8,128)(2,1)S(1)}, bf16[32,24,128]{2,1,0:T(8,128)(2,1)S(1)}, u32[]{:S(2)}, u32[]{:S(2)}) collective-permute-start(bf16[32,24,128]{2,1,0:T(8,128)(2,1)S(1)} %slice.4.w0), channel_id=1, source_target_pairs={{0,24},{8,0},{16,8},{24,16},{32,56},{40,32},{48,40},{56,48},{64,88... | collective-permute-start | bytes 589832 | tf_op jit(solution)/shard_map/ppermute | solution.py:281
  64.2 9.4 %collective-permute-start.1 = (bf16[32,24,128]{2,1,0:T(8,128)(2,1)S(1)}, bf16[32,24,128]{2,1,0:T(8,128)(2,1)}, u32[]{:S(2)}, u32[]{:S(2)}) collective-permute-start(bf16[32,24,128]{2,1,0:T(8,128)(2,1)S(1)} %slice.4.w0), channel_id=1, source_target_pairs={{0,16},{8,24},{16,0},{24,8},{32,48},{40,56},{48,32},{56,40},{64,80... | collective-permute-start | bytes 589832 | tf_op jit(solution)/shard_map/ppermute | solution.py:281
  65.7 10.5 %collective-permute-start = (bf16[32,24,128]{2,1,0:T(8,128)(2,1)S(1)}, bf16[32,24,128]{2,1,0:T(8,128)(2,1)}, u32[]{:S(2)}, u32[]{:S(2)}) collective-permute-start(bf16[32,24,128]{2,1,0:T(8,128)(2,1)S(1)} %slice.4.w0), channel_id=1, source_target_pairs={{0,8},{8,16},{16,24},{24,0},{32,40},{40,48},{48,56},{56,32},{64,72... | collective-permute-start | bytes 589832 | tf_op jit(solution)/shard_map/ppermute | solution.py:281
  69.5 12.0 %all-to-all-start.3 = ((f32[8,8,128]{2,1,0:T(8,128)}), f32[8,8,128]{2,1,0:T(8,128)S(1)}, u32[]{:S(2)}, u32[]{:S(2)}) async-start(f32[8,8,128]{2,1,0:T(8,128)} %shard_map.199), calls=%async_computation.3 | async-start | bytes 65536 | tf_op jit(solution)/shard_map/all_to_all | solution.py:21
  73.2 2.9 %copy-start.10 = (bf16[32,24,128]{2,1,0:T(8,128)(2,1)}, bf16[32,24,128]{2,1,0:T(8,128)(2,1)S(1)}, u32[]{:S(2)}) copy-start(bf16[32,24,128]{2,1,0:T(8,128)(2,1)S(1)} %collective-permute-done.2.w3) | copy-start | bytes 589828
  78.5 3.0 %copy-start.2 = (bf16[192,512]{1,0:T(8,128)(2,1)S(1)}, bf16[192,512]{1,0:T(8,128)(2,1)}, u32[]{:S(2)}) copy-start(bf16[192,512]{1,0:T(8,128)(2,1)} %get-tuple-element.27.whole_q_t) | copy-start | bytes 589828
  78.5 3.0 %copy-start.3 = (f32[32,256]{1,0:T(8,128)S(1)}, f32[32,256]{1,0:T(8,128)}, u32[]{:S(2)}) copy-start(f32[32,256]{1,0:T(8,128)} %wo.3) | copy-start | bytes 98308
  78.5 3.1 %copy-start.4 = (f32[16,192]{1,0:T(8,128)S(1)}, f32[16,192]{1,0:T(8,128)}, u32[]{:S(2)}) copy-start(f32[16,192]{1,0:T(8,128)} %wq.3) | copy-start | bytes 36868
  81.6 1.0 %copy-start.1 = (bf16[1024,256]{1,0:T(8,128)(2,1)S(1)}, bf16[1024,256]{1,0:T(8,128)(2,1)}, u32[]{:S(2)}) copy-start(bf16[1024,256]{1,0:T(8,128)(2,1)} %get-tuple-element.28.whole_o) | copy-start | bytes 1572868
